TPU v7x, 256 devices: a whole 4x4x8 slice. The times are simulated.
256 devices in a mesh: sp: 32 (over z, y), fs: 4 (over x), tp: 2 (over core).
Axes of the slice: x: 4, y: 4, z: 8, core: 2. Of those that a mesh axis runs over, the one named last changes fastest.
Arguments:
- tokens: bfloat16 [4, 4096, 2048], P('fs', ('sp', 'tp')), may hold values from -6 to 6
- norm_gain: float32 [2048], replicated, may hold values from 0.1 to 1.9
- drive_weight: bfloat16 [2048, 1024], P('fs', 'tp'), may hold values from -0.125 to 0.125
- query_weight: bfloat16 [2048, 1024], P('fs', 'tp'), may hold values from -1 to 1
- key_weight: bfloat16 [2048, 1024], P('fs', 'tp'), may hold values from -1 to 1
- value_weight: bfloat16 [2048, 1024], P('fs', 'tp'), may hold values from -0.5 to 0.5
- key_offset: bfloat16 [8, 4, 4096], P('tp', 'fs', 'sp'), may hold values from -16 to 0
- log_step: float32 [64], P('tp'), may hold values from -4.7 to -1.2
- lambda_real: float32 [64, 64], P('tp'), as said below
- lambda_imag: float32 [64, 64], P('tp'), may hold values from 1 to 201
- input_map: float32 [2, 64, 64, 16], P(None, 'tp'), may hold values from -2 to 2
- output_map: float32 [2, 64, 16, 64], P(None, 'tp'), may hold values from -0.5 to 0.5
- skip_gain: float32 [1024], P('tp'), may hold values from -5 to 5
- forget: float32 [64, 4, 4096], P('tp', 'fs', 'sp'), may hold values from -0.52 to 0
- initial_state: float32 [2, 4, 64, 64], P(None, 'fs', 'tp'), may hold values from -24 to 24
- scan_out_weight: bfloat16 [1024, 2048], P('tp', 'fs'), may hold values from -0.125 to 0.125
- attend_out_weight: bfloat16 [1024, 2048], P('tp', 'fs'), may hold values from -0.125 to 0.125
Outputs:
- layer_out: bfloat16 [4, 4096, 2048], P('fs', ('sp', 'tp'))
Inputs may be any that keep to these rules, and one draw needn't show every extreme that they name: lambda_real[g, n] * exp(log_step[g]) lies between -1/30 and 0 for every group g and state n.
All inputs are finite; a program needn't handle non-finite values.
Results may differ from a plain program's by a relative error of at most 0.009.
Values may be sent and summed in bfloat16 or wider, within the bound.
A program may use at most 128 MiB of HBM per device.

v0:
```python
import math

import jax
import jax.numpy as jnp
from jax import lax
from jax.sharding import Mesh
from jax.sharding import PartitionSpec as P

HEAD_DIM = 128
SP = ("sp_0", "sp_1")
SP_TP = ("sp_0", "sp_1", "tp")


epsilon = 1e-06


def in_blocks(shard, dim, devices):
    dims = shard.shape
    blocks = shard.reshape(*dims[:dim], devices, dims[dim] // devices, *dims[dim + 1 :])
    return jnp.moveaxis(blocks, dim, 0)


def sum_at_owner(shard, axis, dim):
    blocks = in_blocks(shard, dim, lax.axis_size(axis))
    arrived = lax.all_to_all(blocks, axis, split_axis=0, concat_axis=0, tiled=True)
    return arrived.sum(axis=0)


def filled_with(shard, identity):
    return jax.tree.map(
        lambda part, zero: jnp.zeros_like(part) + jnp.asarray(zero, part.dtype), shard, identity
    )


def gathered_once(shard, axis):
    leaves = jax.tree.leaves(shard)
    order = sorted(range(len(leaves)), key=lambda k: -leaves[k].size)
    width = (1, *leaves[order[0]].shape)[-1]
    lines = [
        jnp.pad(leaves[k].reshape(-1), (0, -leaves[k].size % width)).reshape(-1, width)
        for k in order
    ]
    both, at, found = (lax.all_gather(jnp.concatenate(lines), axis), 0, {})
    for k, line in zip(order, lines):
        section = both[:, at : at + len(line)].reshape(len(both), -1)
        found[k] = section[:, : leaves[k].size].reshape(-1, *leaves[k].shape)
        at += len(line)
    numbers = iter(range(len(leaves)))
    return jax.tree.map(lambda _: found[next(numbers)], shard)


def entering(shard, axes, combine, identity):
    before = start = filled_with(shard, identity)
    so_far = shard
    for axis in reversed(axes):
        devices, index = (lax.axis_size(axis), lax.axis_index(axis))
        pieces = gathered_once(so_far, axis)
        inside, so_far = (start, start)
        for k in range(devices):
            passed = k < index
            so_far = combine(so_far, jax.tree.map(lambda part: part[k], pieces))
            inside = jax.tree.map(lambda new, old: jnp.where(passed, new, old), so_far, inside)
        before = combine(inside, before)
    return before


def sent_together(arrays, axis, dim, along):
    widths = [math.prod(a.shape[along:]) for a in arrays]
    both = jnp.concatenate(
        [a.reshape(*a.shape[:along], w) for a, w in zip(arrays, widths)], axis=along
    )
    whole = lax.all_gather(both, axis, axis=dim, tiled=True)
    blocks = jnp.split(whole, [sum(widths[:k]) for k in range(1, len(widths))], axis=along)
    return tuple(
        (b.reshape(*whole.shape[:along], *a.shape[along:]) for a, b in zip(arrays, blocks))
    )


def sent_and_summed(shard, axis, dim):
    devices = lax.axis_size(axis)
    blocks = lax.all_to_all(in_blocks(shard, dim, devices), axis, 0, 0, tiled=True)
    return jnp.sum(blocks.astype(jnp.float32), axis=0)


def complex_mul(left_real, left_imag, right_real, right_imag):
    return (
        left_real * right_real - left_imag * right_imag,
        left_real * right_imag + left_imag * right_real,
    )


def chain_combine(earlier, later):
    gain_real, gain_imag = complex_mul(later[0], later[1], earlier[0], earlier[1])
    moved_real, moved_imag = complex_mul(later[0], later[1], earlier[2], earlier[3])
    return (gain_real, gain_imag, moved_real + later[2], moved_imag + later[3])


def normalize(token_rows, norm_gain):
    values = token_rows.astype(jnp.float32)
    return (
        values
        * lax.rsqrt(jnp.mean(values * values, axis=1, keepdims=True) + epsilon)
        * norm_gain[None]
    ).astype(jnp.bfloat16)


def scan_local(inputs, forget_rows, log_step, lambda_real, lambda_imag, input_map):
    length_dev, groups, _ = inputs.shape
    states = lambda_real.shape[1]
    state_width = groups * states
    highest = lax.Precision.DEFAULT
    step_size = jnp.exp(log_step)[:, None]
    log_gain = lambda_real * step_size
    rotate = lambda_imag * step_size
    magnitude = jnp.exp(log_gain)
    bar_real = magnitude * jnp.cos(rotate)
    bar_imag = magnitude * jnp.sin(rotate)
    divisor = lambda_real * lambda_real + lambda_imag * lambda_imag
    shifted = bar_real - 1.0
    factor_real = (shifted * lambda_real + bar_imag * lambda_imag) / divisor
    factor_imag = (bar_imag * lambda_real - shifted * lambda_imag) / divisor
    map_real = factor_real[:, :, None] * input_map[0] - factor_imag[:, :, None] * input_map[1]
    map_imag = factor_real[:, :, None] * input_map[1] + factor_imag[:, :, None] * input_map[0]
    drive_real = jnp.einsum("tgc,gnc->tgn", inputs, map_real, precision=highest)
    drive_imag = jnp.einsum("tgc,gnc->tgn", inputs, map_imag, precision=highest)
    span_len = math.gcd(length_dev, 64)
    blocks = length_dev // span_len
    drive_real = drive_real.reshape(blocks, span_len, state_width)
    drive_imag = drive_imag.reshape(blocks, span_len, state_width)
    cum_forget = jnp.cumsum(forget_rows.T.reshape(blocks, span_len, groups), axis=1)
    ladder = jnp.arange(1, span_len + 1, dtype=jnp.float32)
    log_rel = (
        cum_forget[:, :, :, None] + ladder[None, :, None, None] * log_gain[None, None]
    ).reshape(blocks, span_len, state_width)
    angles = (ladder[:, None, None] * rotate[None]).reshape(1, span_len, state_width)
    cosine = jnp.cos(angles)
    sine_part = jnp.sin(angles)
    rel_mag = jnp.exp(log_rel)
    inv_mag = jnp.exp(-log_rel)
    rel_real = rel_mag * cosine
    rel_imag = rel_mag * sine_part
    scaled_real, scaled_imag = complex_mul(
        drive_real, drive_imag, inv_mag * cosine, -inv_mag * sine_part
    )
    local_real, local_imag = complex_mul(
        rel_real, rel_imag, jnp.cumsum(scaled_real, axis=1), jnp.cumsum(scaled_imag, axis=1)
    )

    def advance(running, element):
        state_real, state_imag = complex_mul(element[2], element[3], running[0], running[1])
        gain_real, gain_imag = complex_mul(element[2], element[3], running[2], running[3])
        return ((state_real + element[0], state_imag + element[1], gain_real, gain_imag), running)

    zeros_row = jnp.zeros((state_width,), jnp.float32)
    initial = (zeros_row, zeros_row, jnp.ones((state_width,), jnp.float32), zeros_row)
    summary, before = lax.scan(
        advance, initial, (local_real[:, -1], local_imag[:, -1], rel_real[:, -1], rel_imag[:, -1])
    )
    return ((local_real, local_imag, rel_real, rel_imag, before), summary)


def scan_finish(pieces, carry_real, carry_imag, inputs, output_map, skip_gain):
    local_real, local_imag, rel_real, rel_imag, before = pieces
    length_dev, groups, channels = inputs.shape
    added_real, added_imag = complex_mul(before[2], before[3], carry_real[None], carry_imag[None])
    enter_real = before[0] + added_real
    enter_imag = before[1] + added_imag
    lift_real, lift_imag = complex_mul(rel_real, rel_imag, enter_real[:, None], enter_imag[:, None])
    state_real = (local_real + lift_real).reshape(length_dev, groups, -1)
    state_imag = (local_imag + lift_imag).reshape(length_dev, groups, -1)
    highest = lax.Precision.DEFAULT
    readout = jnp.einsum("tgn,gcn->tgc", state_real, output_map[0], precision=highest)
    readout = readout - jnp.einsum("tgn,gcn->tgc", state_imag, output_map[1], precision=highest)
    readout = readout + skip_gain.reshape(groups, channels)[None] * inputs
    return jax.nn.gelu(readout).reshape(length_dev, groups * channels).astype(jnp.bfloat16)


def on_device(
    tokens,
    norm_gain,
    drive_weight,
    query_weight,
    key_weight,
    value_weight,
    key_offset,
    log_step,
    lambda_real,
    lambda_imag,
    input_map,
    output_map,
    skip_gain,
    forget,
    initial_state,
    scan_out_weight,
    attend_out_weight,
):
    normed_own = normalize(tokens[0], norm_gain)
    normed_block = lax.all_gather(normed_own, "tp", axis=0, tiled=True)
    sliced = lax.all_to_all(normed_block, "fs", split_axis=1, concat_axis=0, tiled=True)
    stacked = jnp.concatenate((drive_weight, query_weight, key_weight, value_weight), axis=1)
    projected = sum_at_owner(
        jnp.dot(sliced, stacked, preferred_element_type=jnp.float32), "fs", 0
    ).astype(jnp.bfloat16)
    length_dev = projected.shape[0]
    branch = drive_weight.shape[1]
    groups = log_step.shape[0]
    head_count = query_weight.shape[1] // HEAD_DIM
    inputs = projected[:, :branch].astype(jnp.float32).reshape(length_dev, groups, -1)
    queries = projected[:, branch : 2 * branch].reshape(length_dev, head_count, HEAD_DIM)
    key_own = projected[:, 2 * branch : 3 * branch].reshape(length_dev, head_count, HEAD_DIM)
    value_own = projected[:, 3 * branch :].reshape(length_dev, head_count, HEAD_DIM)
    pieces, summary = scan_local(
        inputs, forget[:, 0, :], log_step, lambda_real, lambda_imag, input_map
    )
    init_real = initial_state[0, 0].reshape(-1)
    init_imag = initial_state[1, 0].reshape(-1)
    position = lax.axis_index(SP)
    devices = lax.axis_size(SP)
    ones_row = jnp.ones_like(init_real)
    zeros_row = jnp.zeros_like(init_real)
    prefix = entering(
        (summary[2], summary[3], summary[0], summary[1]),
        SP,
        chain_combine,
        (ones_row, zeros_row, zeros_row, zeros_row),
    )
    pushed_real, pushed_imag = complex_mul(prefix[0], prefix[1], init_real, init_imag)
    carry_real = prefix[2] + pushed_real
    carry_imag = prefix[3] + pushed_imag
    query_place = position * length_dev + jnp.arange(length_dev, dtype=jnp.int32)
    offset_own = key_offset[:, 0, :]
    empty_state = (
        jnp.zeros((length_dev, head_count, HEAD_DIM), jnp.float32),
        jnp.zeros((length_dev, head_count), jnp.float32),
    )
    every_key, every_value, every_offset = sent_together(
        (key_own, value_own, offset_own.T), SP, 0, 2
    )
    span_blocks = math.gcd(devices, max(1, 524288 // (length_dev * length_dev)))
    span_keys = span_blocks * length_dev
    group_total = devices // span_blocks

    def advance_group(turn, running):
        summed_now, fallen = running
        begin_row = (group_total - 1 - turn) * span_keys
        value_group = every_value.reshape(span_blocks, length_dev, head_count, HEAD_DIM)
        offset_group = every_offset.T
        product = jnp.einsum("qhd,khd->qhk", queries, every_key, preferred_element_type=jnp.float32)
        scores = (product * HEAD_DIM ** (-0.5) + offset_group.astype(jnp.float32)[None]).reshape(
            length_dev, head_count, span_blocks, length_dev
        )
        key_place = begin_row + jnp.arange(span_keys, dtype=jnp.int32)
        visible = (key_place[None, :] < query_place[:, None]).reshape(
            length_dev, 1, span_blocks, length_dev
        )
        escape_log = jnp.where(visible, jax.nn.log_sigmoid(-scores), 0.0)
        behind_log = lax.cumsum(escape_log, axis=3, reverse=True) - escape_log
        block_sum = jnp.sum(escape_log, axis=3)
        after_log = lax.cumsum(block_sum, axis=2, reverse=True) - block_sum
        weight = jnp.where(visible, jnp.exp(jax.nn.log_sigmoid(scores) + behind_log), 0.0).astype(
            jnp.bfloat16
        )
        portion = jnp.einsum(
            "qhck,ckhd->qhcd", weight, value_group, preferred_element_type=jnp.float32
        )
        scaled = jnp.sum(jnp.exp(fallen[:, :, None] + after_log)[..., None] * portion, axis=2)
        return (summed_now + scaled, fallen + jnp.sum(block_sum, axis=2))

    attended = lax.fori_loop(0, group_total, advance_group, empty_state)
    scan_out = scan_finish(pieces, carry_real, carry_imag, inputs, output_map, skip_gain)
    attend_out = attended[0].astype(jnp.bfloat16).reshape(length_dev, -1)
    out_scan, out_attend = (
        lax.all_gather(scan_out_weight, "fs", axis=1, tiled=True),
        lax.all_gather(attend_out_weight, "fs", axis=1, tiled=True),
    )
    summed = sent_and_summed(
        (
            jnp.dot(scan_out, out_scan, preferred_element_type=jnp.float32)
            + jnp.dot(attend_out, out_attend, preferred_element_type=jnp.float32)
        ).astype(jnp.bfloat16),
        "tp",
        0,
    )
    return summed.astype(jnp.bfloat16)[None]


def solution(mesh):
    split = Mesh(
        mesh.devices.reshape(8, 4, mesh.shape["fs"], mesh.shape["tp"]), ("sp_0", "sp_1", "fs", "tp")
    )
    in_specs = (
        P("fs", SP_TP, None),
        P(),
        P("fs", "tp"),
        P("fs", "tp"),
        P("fs", "tp"),
        P("fs", "tp"),
        P("tp", "fs", SP),
        P("tp"),
        P("tp", None),
        P("tp", None),
        P(None, "tp", None, None),
        P(None, "tp", None, None),
        P("tp"),
        P("tp", "fs", SP),
        P(None, "fs", "tp", None),
        P("tp", "fs"),
        P("tp", "fs"),
    )
    out_specs = P("fs", SP_TP, None)
    return jax.shard_map(
        on_device, mesh=split, in_specs=in_specs, out_specs=out_specs, check_vma=False
    )
```

profile of v0, /device:TPU:1, one launch (start us, length us, event | category | flops | bytes accessed | tf_op | source)
XLA Modules:
  0.0 306.0 jit_solution(3060473555840659280)
XLA Ops:
  8.9 5.0 %all_gather.24 = bf16[128,2048]{1,0:T(8,128)(2,1)S(1)} all-gather(bf16[64,2048]{1,0:T(8,128)(2,1)S(1)} %fusion.42), channel_id=1, replica_groups=mesh['sp_0'=8,'sp_1'=4,'fs'=4,'tp'=2] {'tp'}, dimensions={0}, use_global_device_ids=true | all-gather | bytes 786432 | tf_op jit(solution)/shard_map/all_gather | solution.py:198
  14.4 11.6 %all_to_all.26 = bf16[128,4,512]{2,0,1:T(8,128)(2,1)S(1)} all-to-all(bf16[128,4,512]{2,0,1:T(8,128)(2,1)S(1)} %copy.70), channel_id=1, replica_groups=mesh['sp_0'=8,'sp_1'=4,'fs'=4,'tp'=2] {'fs'}, dimensions={1} | all-to-all | bytes 1048576 | tf_op jit(solution)/shard_map/all_to_all | solution.py:199
  26.0 3.3 %fusion.14 = f32[4,128,2048]{2,1,0:T(8,128)} fusion(bf16[512,512]{1,0:T(8,128)(2,1)S(1)} %copy-done.20, bf16[512,512]{1,0:T(8,128)(2,1)S(1)} %copy-done.21, bf16[512,512]{1,0:T(8,128)(2,1)S(1)} %copy-done.22, bf16[512,512]{1,0:T(8,128)(2,1)S(1)} %copy-done.23, bf16[128,4,512]{2,0,1:T(8,128)(2,1)S(1)} %all_to_all.26), kind=kOutput, calls=%fused_computation.31 | convolution fusion | flops 1082130432 | bytes 6815744 | tf_op jit(solution)/shard_map/dot_general | solution.py:202
  29.3 5.0 %all-to-all-start.1 = ((f32[4,128,2048]{2,1,0:T(8,128)}), f32[4,128,2048]{2,1,0:T(8,128)}, u32[]{:S(2)}, u32[]{:S(2)}) async-start(f32[4,128,2048]{2,1,0:T(8,128)} %fusion.14), calls=%async_computation.1 | async-start | bytes 8388608 | tf_op jit(solution)/shard_map/all_to_all | solution.py:25
  35.4 63.6 %all-to-all-done.1 = f32[4,128,2048]{2,1,0:T(8,128)} async-done(((f32[4,128,2048]{2,1,0:T(8,128)}), f32[4,128,2048]{2,1,0:T(8,128)}, u32[]{:S(2)}, u32[]{:S(2)}) %all-to-all-start.1) | async-done | bytes 4194336 | tf_op jit(solution)/shard_map/all_to_all | solution.py:25
  98.9 2.6 reduce_sum.56
  105.3 2.9 copy.66
  112.7 3.0 add.930
  120.9 3.0 add.922
  125.0 3.0 mul.1600
  129.2 3.0 mul.1627
  136.2 2.5 convolution_bitcast_fusion
  138.7 2.4 convolution_bitcast_fusion.1
  141.1 2.5 reshape.1686
  143.6 2.1 copy.100
  145.8 2.5 reshape.1685
  148.2 2.3 copy.98
  150.5 4.1 %multiply_subtract_fusion.1 = (f32[2,64,2048]{2,1,0:T(8,128)S(1)}, f32[2,64,2048]{2,1,0:T(8,128)}, f32[2,64,2048]{2,1,0:T(8,128)}, f32[2,64,2048]{2,1,0:T(8,128)}) fusion(f32[2,64,2048]{2,1,0:T(8,128)} %copy.100, f32[2,64,2048]{2,1,0:T(8,128)} %copy.98, f32[2,64,2048]{2,1,0:T(8,128)} %add.930, f32[64,2048]{1,0:T(8,128)S(1)} %get-tuple-element.285, ...), kind=kLoop, calls=%fused_computation.58 | loop fusion | flops 3407872 | bytes 8912896 | tf_op jit(solution)/shard_map/sub | solution.py:87
  160.4 11.4 %all-gather.2 = f32[4,4,2048]{2,1,0:T(4,128)S(1)} all-gather(f32[1,4,2048]{2,1,0:T(4,128)S(1)} %maximum_bitcast_fusion.2), channel_id=2, replica_groups=mesh['sp_0'=8,'sp_1'=4,'fs'=4,'tp'=2] {'sp_1'}, dimensions={0}, use_global_device_ids=true | all-gather | bytes 163840 | tf_op jit(solution)/shard_map/all_gather | solution.py:43
  172.1 25.2 %all-gather.3 = f32[8,4,2048]{2,1,0:T(4,128)S(1)} all-gather(f32[1,4,2048]{2,1,0:T(4,128)S(1)} %maximum_bitcast_fusion.3), channel_id=3, replica_groups=mesh['sp_0'=8,'sp_1'=4,'fs'=4,'tp'=2] {'sp_0'}, dimensions={0}, use_global_device_ids=true | all-gather | bytes 294912 | tf_op jit(solution)/shard_map/all_gather | solution.py:43
  197.6 2.2 reduce_window_sum.59
  199.8 2.2 reduce_window_sum.61
  202.3 2.1 mul.1765
  204.5 2.2 mul.1770
  206.9 5.8 %subtract_add_fusion.1 = (bf16[128,32,64]{2,1,0:T(8,128)(2,1)S(1)}, bf16[128,32,64]{2,1,0:T(8,128)(2,1)S(1)}) fusion(f32[128,32,64]{2,1,0:T(8,128)} %mul.1770, f32[128,32,64]{2,1,0:T(8,128)} %mul.1765, f32[128,32,64]{2,1,0:T(8,128)} %reduce_window_sum.61, f32[128,32,64]{2,1,0:T(8,128)} %reduce_window_sum.59, f32[128,32,64]{2,1,0:T(8,128)} %mul.1600, ...), kind=kLoop, calls=%fused_computation.43 | loop fusion | flops 4980736 | bytes 8404992 | tf_op jit(solution)/shard_map/add | solution.py:169
  216.1 9.8 %all-gather.10.cloned.1.call-done = bf16[4096,4,257]{2,0,1:T(8,128)(2,1)} async-done(((bf16[128,4,257]{2,0,1:T(8,128)(2,1)}), bf16[4096,4,257]{2,0,1:T(8,128)(2,1)}) %all-gather.10.cloned.1.call-update) | async-done | bytes 8421392 | tf_op jit(solution)/shard_map/all_gather | solution.py:72
  225.9 3.5 %convert_reduce_fusion = f32[4096,4]{0,1:T(4,128)S(1)} fusion(bf16[4096,4,257]{2,0,1:T(8,128)(2,1)} %all-gather.10.cloned.1.call-done), kind=kLoop, calls=%fused_computation.23 | loop fusion | flops 16384 | bytes 98304 | tf_op jit(solution)/shard_map/while/body/eval_jaxpr/convert_element_type | solution.py:249
  229.4 7.3 %multiply_add_fusion.1 = f32[4,4096,128]{2,1,0:T(8,128)S(1)} fusion(bf16[128,4,128]{0,2,1:T(8,128)(2,1)S(1)} %bitcast.378, bf16[4096,4,257]{2,0,1:T(8,128)(2,1)} %all-gather.10.cloned.1.call-done, f32[4,4096]{1,0:T(4,128)S(1)} %bitcast.372), kind=kOutput, calls=%fused_computation.24 | convolution fusion | flops 541065216 | bytes 12779520 | tf_op jit(solution)/shard_map/while/body/eval_jaxpr/qhd,khd->qhk/dot_general | solution.py:248
  236.7 45.8 %fusion.6 = (bf16[128,4,32,128]{0,2,1,3:T(8,128)(2,1)}, f32[128,4,32]{0,2,1:T(8,128)S(1)}) fusion(f32[128,4,32,128]{0,3,2,1:T(8,128)S(1)} %bitcast.359, pred[128,32,128]{0,1,2:T(8,128)(4,1)S(1)} %copy-done.2), kind=kOutput, calls=%fused_computation.20 | output fusion | flops 327139328 | bytes 13172736 | tf_op jit(solution)/shard_map/while/body/eval_jaxpr/reduce_window_sum | solution.py:257
  282.6 2.2 slice-done
  286.1 4.8 %fusion.7 = bf16[128,4,128]{0,2,1:T(8,128)(2,1)S(1)} fusion(f32[128,4,32]{0,2,1:T(8,128)S(1)} %copy.92, bf16[32,128,4,128]{3,1,0,2:T(8,128)(2,1)S(1)} %bitcast.358, bf16[128,4,32,128]{0,2,1,3:T(8,128)(2,1)S(1)} %copy-done.25), kind=kOutput, calls=%fused_computation.22 | convolution fusion | flops 540999680 | bytes 8585216 | tf_op jit(solution)/shard_map/while/body/eval_jaxpr/qhck,ckhd->qhcd/dot_general | solution.py:263
  293.0 5.4 %all_to_all.27 = bf16[2,64,2048]{2,1,0:T(8,128)(2,1)S(1)} all-to-all(bf16[2,64,2048]{2,1,0:T(8,128)(2,1)S(1)} %bitcast.367), channel_id=1, replica_groups=mesh['sp_0'=8,'sp_1'=4,'fs'=4,'tp'=2] {'tp'}, dimensions={0} | all-to-all | bytes 1048576 | tf_op jit(solution)/shard_map/all_to_all | solution.py:81
  (150 shorter events, 38.6 us)
Async XLA Ops:
  6.5 19.5 %copy-start.23 = (bf16[512,512]{1,0:T(8,128)(2,1)S(1)}, bf16[512,512]{1,0:T(8,128)(2,1)}, u32[]{:S(2)}) copy-start(bf16[512,512]{1,0:T(8,128)(2,1)} %param.21) | copy-start | bytes 1572868
  6.5 19.5 %copy-start.22 = (bf16[512,512]{1,0:T(8,128)(2,1)S(1)}, bf16[512,512]{1,0:T(8,128)(2,1)}, u32[]{:S(2)}) copy-start(bf16[512,512]{1,0:T(8,128)(2,1)} %param.22) | copy-start | bytes 1572868
  6.5 19.5 %copy-start.21 = (bf16[512,512]{1,0:T(8,128)(2,1)S(1)}, bf16[512,512]{1,0:T(8,128)(2,1)}, u32[]{:S(2)}) copy-start(bf16[512,512]{1,0:T(8,128)(2,1)} %param.23) | copy-start | bytes 1572868
  6.5 19.5 %copy-start.20 = (bf16[512,512]{1,0:T(8,128)(2,1)S(1)}, bf16[512,512]{1,0:T(8,128)(2,1)}, u32[]{:S(2)}) copy-start(bf16[512,512]{1,0:T(8,128)(2,1)} %param.24) | copy-start | bytes 1572868
  29.3 5.8 %copy-start.18 = (bf16[4,1,128]{2,0,1:T(4,128)(2,1)S(1)}, bf16[4,1,128]{2,0,1:T(4,128)(2,1)}, u32[]{:S(2)}) copy-start(bf16[4,1,128]{2,0,1:T(4,128)(2,1)} %param.25) | copy-start | bytes 3076
  29.3 69.6 %all-to-all-start.1 = ((f32[4,128,2048]{2,1,0:T(8,128)}), f32[4,128,2048]{2,1,0:T(8,128)}, u32[]{:S(2)}, u32[]{:S(2)}) async-start(f32[4,128,2048]{2,1,0:T(8,128)} %fusion.14), calls=%async_computation.1 | async-start | bytes 8388608 | tf_op jit(solution)/shard_map/all_to_all | solution.py:25
  34.3 179.7 %all-gather.8.cloned.1.call-start = ((), (), s32[]{:S(2)}) async-start(), calls=%async_computation.3 | async-start | bytes 2621440 | tf_op jit(solution)/shard_map/all_gather | solution.py:273
  35.1 190.8 %all-gather.10.cloned.1.call-start = ((), (), s32[]{:S(2)}) async-start(), calls=%async_computation.4 | async-start | bytes 12976128 | tf_op jit(solution)/shard_map/all_gather | solution.py:72
  35.3 69.0 %copy-start.24 = (f32[32]{0:T(128)S(1)}, f32[32]{0:T(128)}, u32[]{:S(2)}) copy-start(f32[32]{0:T(128)} %param.26) | copy-start | bytes 388
  35.3 69.0 %copy-start.15 = (f32[32,64]{1,0:T(8,128)S(1)}, f32[32,64]{1,0:T(8,128)}, u32[]{:S(2)}) copy-start(f32[32,64]{1,0:T(8,128)} %param.28) | copy-start | bytes 24580
  35.3 69.0 %copy-start.16 = (f32[32,64]{1,0:T(8,128)S(1)}, f32[32,64]{1,0:T(8,128)}, u32[]{:S(2)}) copy-start(f32[32,64]{1,0:T(8,128)} %param.27) | copy-start | bytes 24580
  35.3 69.9 %copy-start.9 = (f32[32,1,128]{2,1,0:T(1,128)S(1)}, f32[32,1,128]{2,1,0:T(1,128)}, u32[]{:S(2)}) copy-start(f32[32,1,128]{2,1,0:T(1,128)} %param.32) | copy-start | bytes 49156
  103.0 187.9 %all-gather.12.cloned.1.call-start = ((), (), s32[]{:S(2)}) async-start(), calls=%async_computation.5 | async-start | bytes 2621440 | tf_op jit(solution)/shard_map/all_gather | solution.py:274
  110.0 5.7 %copy-start.8 = (f32[2,1,32,64]{3,2,1,0:T(8,128)S(1)}, f32[2,1,32,64]{3,2,1,0:T(8,128)}, u32[]{:S(2)}) copy-start(f32[2,1,32,64]{3,2,1,0:T(8,128)} %param.33) | copy-start | bytes 49156
  110.0 7.1 %copy-start.19 = (f32[64]{0:T(128)S(1)}, f32[64]{0:T(128)}, u32[]{:S(2)}) copy-start(f32[64]{0:T(128)} %iota_add_fusion.1) | copy-start | bytes 772
  119.0 0.8 copy-start.1
  128.0 5.5 %copy-start.17 = (f32[512]{0:T(512)S(1)}, f32[512]{0:T(512)}, u32[]{:S(2)}) copy-start(f32[512]{0:T(512)} %param.31) | copy-start | bytes 6148
  154.6 4.2 %copy-start.3 = (f32[2048]{0:T(1024)S(1)}, f32[2048]{0:T(1024)}, u32[]{:S(2)}) copy-start(f32[2048]{0:T(1024)} %custom-call) | copy-start | bytes 24580
  154.6 4.3 %copy-start.4 = (f32[2048]{0:T(1024)S(1)}, f32[2048]{0:T(1024)}, u32[]{:S(2)}) copy-start(f32[2048]{0:T(1024)} %custom-call.1) | copy-start | bytes 24580
  154.6 4.3 %copy-start.10 = (f32[2,2048]{1,0:T(2,128)S(1)}, f32[2,2048]{1,0:T(2,128)}, u32[]{:S(2)}) copy-start(f32[2,2048]{1,0:T(2,128)} %custom-call.4) | copy-start | bytes 49156
  154.6 4.3 %copy-start.11 = (f32[2,2048]{1,0:T(2,128)S(1)}, f32[2,2048]{1,0:T(2,128)}, u32[]{:S(2)}) copy-start(f32[2,2048]{1,0:T(2,128)} %custom-call.5) | copy-start | bytes 49156
  154.6 4.3 %copy-start.12 = (f32[2,2048]{1,0:T(2,128)S(1)}, f32[2,2048]{1,0:T(2,128)}, u32[]{:S(2)}) copy-start(f32[2,2048]{1,0:T(2,128)} %custom-call.6) | copy-start | bytes 49156
  154.7 4.3 %copy-start.13 = (f32[2,2048]{1,0:T(2,128)S(1)}, f32[2,2048]{1,0:T(2,128)}, u32[]{:S(2)}) copy-start(f32[2,2048]{1,0:T(2,128)} %custom-call.7) | copy-start | bytes 49156
  160.4 41.7 %copy-start.6 = (f32[2048]{0:T(1024)S(1)}, f32[2048]{0:T(1024)}, u32[]{:S(2)}) copy-start(f32[2048]{0:T(1024)} %reshape_squeeze.6) | copy-start | bytes 24580
  160.4 41.7 %copy-start.7 = (f32[2048]{0:T(1024)S(1)}, f32[2048]{0:T(1024)}, u32[]{:S(2)}) copy-start(f32[2048]{0:T(1024)} %reshape_squeeze.7) | copy-start | bytes 24580
  202.2 4.7 %copy-start = (f32[128,32,64]{2,1,0:T(8,128)S(1)}, f32[128,32,64]{2,1,0:T(8,128)}, u32[]{:S(2)}) copy-start(f32[128,32,64]{2,1,0:T(8,128)} %add.922) | copy-start | bytes 3145732
  206.9 5.8 %copy-start.5 = (f32[2,32,16,64]{3,2,1,0:T(8,128)S(1)}, f32[2,32,16,64]{3,2,1,0:T(8,128)}, u32[]{:S(2)}) copy-start(f32[2,32,16,64]{3,2,1,0:T(8,128)} %param.30) | copy-start | bytes 786436
  206.9 6.5 %copy-start.14 = (f32[32,16]{1,0:T(8,128)S(1)}, f32[32,16]{1,0:T(8,128)}, u32[]{:S(2)}) copy-start(f32[32,16]{1,0:T(8,128)} %mul.1776) | copy-start | bytes 6148
  229.4 7.3 %copy-start.2 = (pred[128,32,128]{0,1,2:T(8,128)(4,1)S(1)}, pred[128,32,128]{0,1,2:T(8,128)(4,1)}, u32[]{:S(2)}) copy-start(pred[128,32,128]{0,1,2:T(8,128)(4,1)} %broadcast_compare_fusion) | copy-start | bytes 1572868
  282.6 2.2 slice-start
  282.6 3.5 %copy-start.25 = (bf16[128,4,32,128]{0,2,1,3:T(8,128)(2,1)S(1)}, bf16[128,4,32,128]{0,2,1,3:T(8,128)(2,1)}, u32[]{:S(2)}) copy-start(bf16[128,4,32,128]{0,2,1,3:T(8,128)(2,1)} %get-tuple-element.210) | copy-start | bytes 12582916
Sparse Core Ops, SparseCore 0:
  37.0 53.6 all-gather.7
  103.1 122.7 all-gather.9
  227.7 30.8 all-gather.11
where the time goes:
time: 311 us; the launch traced here: 306 us
  other arithmetic  78.6 us (25%)
  waiting for transfers between devices  74.7 us (24%)
  blocking collectives  58.6 us (19%)
  local copies, waits for them, and re-layouts  48.6 us (16%)
  matrix products  25.7 us (8%)
  between operations  14 us (5%)
  starting transfers between devices  5.13 us (2%)
    all_to_all x1, waiting for transfers between devices, sum_at_owner(): lax.all_to_all(blocks, axis, split_axis=0, concat_axis=0, tiled=True)  63.6 us
    another operation x1, other arithmetic, advance_group(): behind_log = lax.cumsum(escape_log, axis=3, reverse=True) - escape_log  45.8 us
    all_gather x2, blocking collectives, gathered_once(): both, at, found = (lax.all_gather(jnp.concatenate(lines), axis), 0, {})  36.5 us
    all_to_all x1, blocking collectives, on_device(): lax.all_to_all(normed_block, 'fs', split_axis=1, concat_axis=0, tiled=True)  11.6 us
    add x5, local copies, waits for them, and re-layouts, scan_local(): cum_forget[:, :, :, None]  9.85 us
    all_gather x1, waiting for transfers between devices, sent_together(): whole = lax.all_gather(both, axis, axis=dim, tiled=True)  9.77 us
    dot_general x1, matrix products, advance_group(): jnp.einsum('qhd,khd->qhk', queries, every_key, preferred_element_type=jnp...  7.31 us
  transfers between devices with their start and end apart: 4, of which 2 were waited for; matrix products, arithmetic and copies ran while one was open for 46% of the time, Pallas kernels for 0%

commit v1 on v0

v1 whole, which is shorter than its diff:
```python
import math

import jax
import jax.numpy as jnp
from jax import lax
from jax.experimental import pallas as pl
from jax.experimental.pallas import tpu as pltpu
from jax.sharding import Mesh
from jax.sharding import PartitionSpec as P

SP_TP = ("sp_0", "sp_1", "tp")
SP = ("sp_0", "sp_1")
EPSILON = 1e-06
LOG2E = 1.4426950408889634
NZ, NY, NX, NT = 8, 4, 4, 2
BF16, F32 = jnp.bfloat16, jnp.float32
VMEM = pl.BlockSpec(memory_space=pltpu.VMEM)
MESH_ID = pl.DeviceIdType.MESH


def remote(src, dst, send_sem, recv_sem, where):
    return pltpu.make_async_remote_copy(
        src_ref=src, dst_ref=dst, send_sem=send_sem, recv_sem=recv_sem,
        device_id=where, device_id_type=MESH_ID,
    )


def greet(peers):
    barrier = pltpu.get_barrier_semaphore()
    for peer in peers:
        pl.semaphore_signal(barrier, inc=1, device_id=peer, device_id_type=MESH_ID)


def await_greetings(count):
    pl.semaphore_wait(pltpu.get_barrier_semaphore(), count)


def plane_peers(x, y, t):
    peers = [
        {"fs": (x + dx) % NX, "tp": (t + dt) % NT}
        for dx in range(NX) for dt in range(NT) if (dx, dt) != (0, 0)
    ]
    peers += [
        {"fs": (x + dx) % NX, "sp_1": (y + dy) % NY} for dx in range(NX) for dy in range(1, NY)
    ]
    return peers


def high_low(value):
    high = value.astype(BF16)
    return high, (value - high.astype(F32)).astype(BF16)


def project_kernel(
    tok, gain, w_drive, w_query, w_key, w_value, packed,
    proj, packed_out,
    normed, rows_in, part_out, part_in, packed_in,
    s_rows, r_rows, s_part, r_part, s_packed, r_packed,
):
    y, x, t = (lax.axis_index(a) for a in ("sp_1", "fs", "tp"))
    greet(plane_peers(x, y, t))
    values = tok[...].astype(F32)
    scale = lax.rsqrt(jnp.mean(values * values, axis=1, keepdims=True) + EPSILON)
    rounded = (values * scale * gain[...]).astype(BF16)
    width = rounded.shape[1] // NX
    for k in range(NX):
        normed[k] = rounded[:, k * width : (k + 1) * width]
    half = rounded.shape[0]
    mine = pl.ds(pl.multiple_of(t * half, half), half)
    rows_in[x, mine, :] = normed[x]
    packed_in[y] = packed[y]
    await_greetings(19)
    row_copies = {}
    for dx in (1, 3, 2, 0):
        for dt in range(NT):
            if (dx, dt) != (0, 0):
                to = (x + dx) % NX
                row_copies[dx, dt] = remote(
                    normed.at[to], rows_in.at[x, mine], s_rows.at[dx, dt], r_rows.at[dx, dt],
                    {"fs": to, "tp": (t + dt) % NT},
                )
                row_copies[dx, dt].start()
    packed_copies = []
    for dy in range(1, NY):
        to = (y + dy) % NY
        copy = remote(
            packed.at[to], packed_in.at[y], s_packed.at[dy], r_packed.at[dy], {"sp_1": to}
        )
        copy.start()
        packed_copies.append(copy)
    part_copies = {}
    for dx in (0, 1, 3, 2):
        seq = (x + NX - dx) % NX
        for dt in range(NT):
            if (dx, dt) != (0, 0):
                row_copies[dx, dt].wait_recv()
        rows = rows_in[seq]
        for kind, weight in enumerate((w_drive, w_query, w_key, w_value)):
            product = jnp.dot(rows, weight[...], preferred_element_type=F32).astype(BF16)
            for k in range(NY):
                part_out[dx, k, kind] = product[:, k * 128 : (k + 1) * 128]
        for dy in (1, 3, 2, 0):
            if (dx, dy) != (0, 0):
                to = (y + dy) % NY
                part_copies[dx, dy] = remote(
                    part_out.at[dx, to], part_in.at[dx, dy], s_part.at[dx, dy], r_part.at[dx, dy],
                    {"fs": seq, "sp_1": to},
                )
                part_copies[dx, dy].start()
    part_in[0, 0] = part_out[0, y]
    for copy in packed_copies:
        copy.wait()
    packed_out[...] = packed_in[...]
    for dy in range(NY):
        for dx in range(NX):
            if (dx, dy) != (0, 0):
                part_copies[dx, dy].wait_recv()
        block = (y + NY - dy) % NY
        for kind in range(4):
            total = part_in[0, dy, kind].astype(F32)
            for dx in range(1, NX):
                total = total + part_in[dx, dy, kind].astype(F32)
            proj[kind, block] = total.astype(BF16)
    for copy in row_copies.values():
        copy.wait_send()
    for copy in part_copies.values():
        copy.wait_send()


def project(tok, gain, weights, packed):
    return pl.pallas_call(
        project_kernel,
        out_shape=(
            jax.ShapeDtypeStruct((4, NY, 128, 128), BF16),
            jax.ShapeDtypeStruct((NY, 16, 128), F32),
        ),
        in_specs=[VMEM] * 7,
        out_specs=(VMEM, VMEM),
        scratch_shapes=[
            pltpu.VMEM((NX, 64, 512), BF16),
            pltpu.VMEM((NX, 128, 512), BF16),
            pltpu.VMEM((NX, NY, 4, 128, 128), BF16),
            pltpu.VMEM((NX, NY, 4, 128, 128), BF16),
            pltpu.VMEM((NY, 16, 128), F32),
            pltpu.SemaphoreType.DMA((NX, NT)),
            pltpu.SemaphoreType.DMA((NX, NT)),
            pltpu.SemaphoreType.DMA((NX, NY)),
            pltpu.SemaphoreType.DMA((NX, NY)),
            pltpu.SemaphoreType.DMA((NY,)),
            pltpu.SemaphoreType.DMA((NY,)),
        ],
        compiler_params=pltpu.CompilerParams(
            collective_id=0, has_side_effects=True, vmem_limit_bytes=40 << 20
        ),
        name="project",
    )(tok, gain, *weights, packed)


def attend_pair(query, key, value, offset, fallen, ladder, visible):
    score = lax.dot_general(query, key, (((1,), (1,)), ((), ())), preferred_element_type=F32)
    score = score * (LOG2E * 128**-0.5) + offset
    soft = jnp.maximum(score, 0.0) + LOG2E * jnp.log(1.0 + jnp.exp2(-jnp.abs(score)))
    if visible is not None:
        soft = jnp.where(visible, soft, 0.0)
    sums = jnp.dot(
        jnp.concatenate(high_low(soft), axis=1), ladder, preferred_element_type=F32
    )
    behind = sums[:, :128] if fallen is None else sums[:, :128] + fallen
    weight = jnp.exp2(score + behind)
    if visible is not None:
        weight = jnp.where(visible, weight, 0.0)
    portion = jnp.dot(weight.astype(BF16), value, preferred_element_type=F32)
    total = sums[:, 128:] if fallen is None else sums[:, 128:] + fallen
    return portion, total


def turned(gain, state):
    return gain[0] * state + gain[1] * pltpu.roll(state, 64, 1)


def powers_times(left, right):
    return (
        left[0] * right[0] - left[1] * right[1],
        left[1] * right[0] + left[0] * right[1],
    )


def mix_kernel(
    proj, packed, params, maps,
    attend_out, scan_out,
    right_in, left_in, offset_own, offset_in, state_own, state_in, acc, tot, ladder,
    into_map, out_map, fwd_p, fwd_q, inv_p, inv_q, held, ends, decay,
    s_right, r_right, s_left, r_left, s_offset, r_offset, s_state, r_state,
):
    z, y = lax.axis_index("sp_0"), lax.axis_index("sp_1")
    greet([{"sp_0": (z + dz) % NZ} for dz in range(1, NZ)])
    up, down = {"sp_0": (z + 1) % NZ}, {"sp_0": (z + NZ - 1) % NZ}
    for b in range(NY):
        offset_own[b : b + 1, :] = packed[b, 8:9, :]
        offset_in[0, b : b + 1, :] = packed[b, 8:9, :]
    offset_own[4:8, :] = jnp.zeros((4, 128), F32)
    await_greetings(NZ - 1)
    copies = []

    def send(src, dst, s_sem, r_sem, where):
        copy = remote(src, dst, s_sem, r_sem, where)
        copy.start()
        copies.append(copy)
        return copy

    right, left = {}, {}
    for part in range(2):
        right[1, part] = send(
            proj.at[2 + part], right_in.at[0, part], s_right.at[0, part], r_right.at[0, part], up
        )
        left[1, part] = send(
            proj.at[2 + part], left_in.at[0, part], s_left.at[0, part], r_left.at[0, part], down
        )
    offset_copies = [
        send(
            offset_own, offset_in.at[dz], s_offset.at[dz], r_offset.at[dz], {"sp_0": (z + dz) % NZ}
        )
        for dz in range(1, NZ)
    ]

    row = lax.broadcasted_iota(jnp.int32, (128, 128), 0)
    lane = lax.broadcasted_iota(jnp.int32, (128, 128), 1)

    sign = jnp.where(lane[:8] < 64, -1.0, 1.0)
    lam_real, lam_imag, log_step, initial, skip = (params[y, k] for k in range(5))
    step = jnp.exp(log_step)
    log_gain, rotate = lam_real * step, lam_imag * step
    cosine, sine, magnitude = jnp.cos(rotate), jnp.sin(rotate), jnp.exp(log_gain)
    bar_real, bar_imag = magnitude * cosine, magnitude * sine
    divisor = lam_real * lam_real + lam_imag * lam_imag
    shifted = bar_real - 1.0
    factor_real = (shifted * lam_real + bar_imag * lam_imag) / divisor
    factor_imag = (bar_imag * lam_real - shifted * lam_imag) / divisor * sign
    shrink = jnp.exp(-log_gain)
    gain = (bar_real, sign * bar_imag)
    inverse = (shrink * cosine, -sign * shrink * sine)
    gains, inverses = [gain], [inverse]
    for _ in range(9):
        gains.append(powers_times(gains[-1], gains[-1]))
    for _ in range(6):
        inverses.append(powers_times(inverses[-1], inverses[-1]))
    gain_block, gain_all = gains[7], gains[9]
    gain_last = powers_times(gain_block, inverse)
    into_map[...] = jnp.zeros_like(into_map)
    out_map[...] = jnp.zeros_like(out_map)
    for g in range(8):
        cols, swapped = pl.ds(g * 128, 128), pl.ds(1024 + g * 128, 128)
        raw = maps[y, 0, g]
        entry = factor_real[g : g + 1] * raw + factor_imag[g : g + 1] * pltpu.roll(raw, 64, 1)
        other = pltpu.roll(entry, 64, 1)
        for at in (g * 16, 128 + g * 16):
            into_map[at : at + 16, cols] = entry.astype(BF16)
            into_map[at : at + 16, swapped] = other.astype(BF16)
        raw = maps[y, 1, g]
        out_map[g * 16 : g * 16 + 16, cols] = (raw * -sign[:1]).astype(BF16)
        out_map[g * 16 : g * 16 + 16, swapped] = (pltpu.roll(raw, 64, 1) * -sign[:1]).astype(BF16)
        for table_p, table_q, steps in ((fwd_p, fwd_q, gains), (inv_p, inv_q, inverses)):
            real, imag = jnp.ones((8, 128), F32), jnp.zeros((8, 128), F32)
            for bit in range(3):
                by = tuple(part[g : g + 1] for part in steps[bit])
                new = powers_times((real, imag), by)
                chosen = (row[:8] & (1 << bit)) != 0
                real, imag = jnp.where(chosen, new[0], real), jnp.where(chosen, new[1], imag)
            table_p[:8, cols] = real
            table_q[:8, cols] = imag
            for bit in range(3, 7):
                n = 1 << bit
                by = tuple(part[g : g + 1] for part in steps[bit])
                new = powers_times((table_p[:n, cols], table_q[:n, cols]), by)
                table_p[n : 2 * n, cols] = new[0]
                table_q[n : 2 * n, cols] = new[1]
    until = jnp.where(lane <= row, 1.0, 0.0)
    until_half = until.astype(BF16)
    falls = []
    local = jnp.zeros((8, 128), F32)
    fall_all = jnp.zeros((8, 1), F32)
    for b in range(NY):
        forget = packed[b, :8, :]
        spread = jnp.concatenate(
            [jnp.broadcast_to(forget[g : g + 1], (16, 128)) for g in range(8)], axis=0
        )
        fall = lax.dot_general(
            until, spread, (((1,), (1,)), ((), ())), preferred_element_type=F32,
            precision=lax.Precision.HIGHEST,
        )
        decay[b] = fall
        driven = proj[0, b].astype(F32) * jnp.exp(-fall)
        entered = jnp.dot(
            jnp.concatenate(high_low(driven), axis=1), into_map[...], preferred_element_type=F32
        )
        unturned = entered[:, :1024] * inv_p[...] + entered[:, 1024:] * inv_q[...]
        high, low = high_low(unturned)
        held[b] = jnp.dot(until_half, high, preferred_element_type=F32) + jnp.dot(
            until_half, low, preferred_element_type=F32
        )
        for g in range(8):
            ends[b, g : g + 1, :] = held[b, 127:128, g * 128 : (g + 1) * 128]
        total = jnp.sum(forget, axis=1, keepdims=True)
        falls.append(jnp.exp(total))
        fall_all = fall_all + total
        ends[b] = falls[b] * turned(gain_last, ends[b])
        local = falls[b] * turned(gain_block, local) + ends[b]
    state_own[:8, :] = local
    state_own[8:, :] = jnp.broadcast_to(fall_all, (8, 128))
    state_copies = [
        send(
            state_own, state_in.at[dz], s_state.at[dz], r_state.at[dz], {"sp_0": (z + dz) % NZ}
        )
        for dz in range(1, NZ)
    ]

    ladder_row = lax.broadcasted_iota(jnp.int32, (256, 256), 0) % 128
    ladder_lane = lax.broadcasted_iota(jnp.int32, (256, 256), 1)
    ladder[...] = jnp.where((ladder_lane >= 128) | (ladder_row >= ladder_lane), -1.0, 0.0).astype(
        BF16
    )
    for q in range(NY):
        portion_sum, fallen = None, None
        for k in range(q, -1, -1):
            portion, fallen = attend_pair(
                proj[1, q], proj[2, k], proj[3, k], offset_in[0, k : k + 1, :], fallen,
                ladder[...], lane < row if k == q else None,
            )
            portion_sum = portion if portion_sum is None else portion_sum + portion
        acc[0, q] = portion_sum
        tot[0, q] = fallen

    for copy in offset_copies:
        copy.wait_recv()

    def attend_chunk(dz, key_at, value_at):
        @pl.when(z >= dz)
        def _():
            for q in range(NY):
                acc[dz, q] = jnp.zeros((128, 128), F32)
                tot[dz, q] = jnp.zeros((128, 128), F32)

            def one(turn, carry):
                k = NY - 1 - turn
                key, value = key_at(k), value_at(k)
                offset = offset_in[dz, pl.ds(k, 1), :]
                for q in range(NY):
                    portion, fallen = attend_pair(
                        proj[1, q], key, value, offset, tot[dz, q], ladder[...], None
                    )
                    acc[dz, q] += portion
                    tot[dz, q] = fallen
                return carry

            lax.fori_loop(0, NY, one, 0)

    for i in range(1, 4):
        for part in range(2):
            right[i, part].wait_recv()
            if i < 3 or part == 0:
                right[i + 1, part] = send(
                    right_in.at[i - 1, part], right_in.at[i, part],
                    s_right.at[i, part], r_right.at[i, part], up,
                )
            left[i, part].wait_recv()
            if i < 3 or part == 1:
                left[i + 1, part] = send(
                    left_in.at[i - 1, part], left_in.at[i, part],
                    s_left.at[i, part], r_left.at[i, part], down,
                )
        attend_chunk(i, lambda k: right_in[i - 1, 0, k], lambda k: right_in[i - 1, 1, k])
        attend_chunk(8 - i, lambda k: left_in[i - 1, 0, k], lambda k: left_in[i - 1, 1, k])
    right[4, 0].wait_recv()
    left[4, 1].wait_recv()
    attend_chunk(4, lambda k: right_in[3, 0, k], lambda k: left_in[3, 1, k])
    for dz in range(1, NZ):
        @pl.when(z >= dz)
        def _():
            for q in range(NY):
                fallen = tot[0, q]
                acc[0, q] += jnp.exp2(fallen) * acc[dz, q]
                tot[0, q] = fallen + tot[dz, q]

    for q in range(NY):
        attend_out[q] = acc[0, q].astype(BF16)

    for copy in state_copies:
        copy.wait_recv()
    carry = initial
    for source in range(NZ - 1):
        back = jnp.maximum(z - source, 1)
        arrived = state_in[back]
        moved = jnp.exp(arrived[8:]) * turned(gain_all, carry) + arrived[:8]
        carry = jnp.where(source < z, moved, carry)
    for b in range(NY):
        entering = turned(gain, carry)
        whole = jnp.concatenate(
            [
                held[b, :, g * 128 : (g + 1) * 128] + entering[g : g + 1]
                for g in range(8)
            ],
            axis=1,
        )
        turned_states = jnp.concatenate(
            [(whole * fwd_p[...]).astype(BF16), (whole * fwd_q[...]).astype(BF16)], axis=1
        )
        read = lax.dot_general(
            turned_states, out_map[...], (((1,), (1,)), ((), ())), preferred_element_type=F32
        )
        read = read * jnp.exp(decay[b]) + skip[:1] * proj[0, b].astype(F32)
        inner = math.sqrt(2.0 / math.pi) * (read + 0.044715 * (read * read * read))
        scan_out[b] = (0.5 * read * (1.0 + jnp.tanh(inner))).astype(BF16)
        carry = falls[b] * turned(gain_block, carry) + ends[b]
    for copy in copies:
        copy.wait_send()


def mix(proj, packed, params, maps):
    return pl.pallas_call(
        mix_kernel,
        out_shape=(
            jax.ShapeDtypeStruct((NY, 128, 128), BF16),
            jax.ShapeDtypeStruct((NY, 128, 128), BF16),
        ),
        in_specs=[VMEM] * 4,
        out_specs=(VMEM, VMEM),
        scratch_shapes=[
            pltpu.VMEM((4, 2, NY, 128, 128), BF16),
            pltpu.VMEM((4, 2, NY, 128, 128), BF16),
            pltpu.VMEM((8, 128), F32),
            pltpu.VMEM((NZ, 8, 128), F32),
            pltpu.VMEM((16, 128), F32),
            pltpu.VMEM((NZ, 16, 128), F32),
            pltpu.VMEM((NZ, NY, 128, 128), F32),
            pltpu.VMEM((NZ, NY, 128, 128), F32),
            pltpu.VMEM((256, 256), BF16),
            pltpu.VMEM((256, 2048), BF16),
            pltpu.VMEM((128, 2048), BF16),
            pltpu.VMEM((128, 1024), F32),
            pltpu.VMEM((128, 1024), F32),
            pltpu.VMEM((128, 1024), F32),
            pltpu.VMEM((128, 1024), F32),
            pltpu.VMEM((NY, 128, 1024), F32),
            pltpu.VMEM((NY, 8, 128), F32),
            pltpu.VMEM((NY, 128, 128), F32),
            pltpu.SemaphoreType.DMA((4, 2)),
            pltpu.SemaphoreType.DMA((4, 2)),
            pltpu.SemaphoreType.DMA((4, 2)),
            pltpu.SemaphoreType.DMA((4, 2)),
            pltpu.SemaphoreType.DMA((NZ,)),
            pltpu.SemaphoreType.DMA((NZ,)),
            pltpu.SemaphoreType.DMA((NZ,)),
            pltpu.SemaphoreType.DMA((NZ,)),
        ],
        compiler_params=pltpu.CompilerParams(
            collective_id=1, has_side_effects=True, vmem_limit_bytes=48 << 20
        ),
        name="mix",
    )(proj, packed, params, maps)


def finish_kernel(
    attend, scan, w_attend, w_scan,
    out,
    attend_in, scan_in, part_out, part_in,
    s_attend, r_attend, s_scan, r_scan, s_part, r_part,
):
    y, x, t = (lax.axis_index(a) for a in ("sp_1", "fs", "tp"))
    greet(plane_peers(x, y, t))
    attend_in[0, 0] = attend[y]
    scan_in[0, 0] = scan[y]
    await_greetings(19)
    copies, arriving = [], {}
    for dx in (0, 1, 3, 2):
        for dy in (1, 3, 2, 0):
            if (dx, dy) != (0, 0):
                to = (y + dy) % NY
                where = {"fs": (x + dx) % NX, "sp_1": to}
                pair = (
                    remote(
                        scan.at[to], scan_in.at[dx, dy], s_scan.at[dx, dy], r_scan.at[dx, dy],
                        where,
                    ),
                    remote(
                        attend.at[to], attend_in.at[dx, dy], s_attend.at[dx, dy],
                        r_attend.at[dx, dy], where,
                    ),
                )
                for copy in pair:
                    copy.start()
                    copies.append(copy)
                arriving[dx, dy] = pair
    part_copies = {}
    for dx in (0, 1, 3, 2):
        total = None
        for dy in range(NY):
            for copy in arriving.get((dx, dy), ()):
                copy.wait_recv()
            head = (y + NY - dy) % NY
            rows = pl.ds(pl.multiple_of(head * 128, 128), 128)
            product = jnp.dot(
                attend_in[dx, dy], w_attend[rows, :], preferred_element_type=F32
            ) + jnp.dot(scan_in[dx, dy], w_scan[rows, :], preferred_element_type=F32)
            total = product if total is None else total + product
        rounded = total.astype(BF16)
        for k in range(NT):
            part_out[dx, k] = rounded[k * 64 : (k + 1) * 64]
        for dt in range(NT):
            if (dx, dt) != (0, 0):
                to = (t + dt) % NT
                part_copies[dx, dt] = remote(
                    part_out.at[dx, to], part_in.at[dx, dt], s_part.at[dx, dt], r_part.at[dx, dt],
                    {"fs": (x + NX - dx) % NX, "tp": to},
                )
                part_copies[dx, dt].start()
    part_in[0, 0] = part_out[0, t]
    for dx in (0, 1, 3, 2):
        for dt in range(NT):
            if (dx, dt) != (0, 0):
                part_copies[dx, dt].wait_recv()
        columns = pl.ds(pl.multiple_of((x + dx) % NX * 512, 512), 512)
        out[:, columns] = (part_in[dx, 0].astype(F32) + part_in[dx, 1].astype(F32)).astype(BF16)
    for copy in copies:
        copy.wait_send()
    for copy in part_copies.values():
        copy.wait_send()


def finish(attend, scan, w_attend, w_scan):
    return pl.pallas_call(
        finish_kernel,
        out_shape=jax.ShapeDtypeStruct((64, 2048), BF16),
        in_specs=[VMEM] * 4,
        out_specs=VMEM,
        scratch_shapes=[
            pltpu.VMEM((NX, NY, 128, 128), BF16),
            pltpu.VMEM((NX, NY, 128, 128), BF16),
            pltpu.VMEM((NX, NT, 64, 512), BF16),
            pltpu.VMEM((NX, NT, 64, 512), BF16),
            pltpu.SemaphoreType.DMA((NX, NY)),
            pltpu.SemaphoreType.DMA((NX, NY)),
            pltpu.SemaphoreType.DMA((NX, NY)),
            pltpu.SemaphoreType.DMA((NX, NY)),
            pltpu.SemaphoreType.DMA((NX, NT)),
            pltpu.SemaphoreType.DMA((NX, NT)),
        ],
        compiler_params=pltpu.CompilerParams(
            collective_id=2, has_side_effects=True, vmem_limit_bytes=40 << 20
        ),
        name="finish",
    )(attend, scan, w_attend, w_scan)


def on_device(
    tokens, norm_gain, drive_weight, query_weight, key_weight, value_weight, key_offset, log_step,
    lambda_real, lambda_imag, input_map, output_map, skip_gain, forget, initial_state,
    scan_out_weight, attend_out_weight,
):
    packed = jnp.concatenate(
        [
            forget[:, 0, :].reshape(NY, 8, 128),
            (key_offset[:, 0, :].astype(F32) * LOG2E).reshape(NY, 1, 128),
            jnp.zeros((NY, 7, 128), F32),
        ],
        axis=1,
    )

    def twice(array):
        return jnp.concatenate([array, array], axis=-1).reshape(NY, 8, 128)

    params = jnp.stack(
        [
            twice(lambda_real),
            twice(lambda_imag),
            jnp.broadcast_to(log_step.reshape(NY, 8, 1), (NY, 8, 128)),
            jnp.concatenate([initial_state[0, 0], initial_state[1, 0]], axis=-1).reshape(
                NY, 8, 128
            ),
            jnp.broadcast_to(skip_gain.reshape(NY, 1, 128), (NY, 8, 128)),
        ],
        axis=1,
    )
    maps = jnp.stack(
        [
            jnp.concatenate([input_map[0], input_map[1]], axis=1)
            .transpose(0, 2, 1)
            .reshape(NY, 8, 16, 128),
            jnp.concatenate([output_map[0], output_map[1]], axis=2).reshape(NY, 8, 16, 128),
        ],
        axis=1,
    )
    weights = (drive_weight, query_weight, key_weight, value_weight)
    proj, packed_all = project(tokens[0], norm_gain[None], weights, packed)
    attend, scan = mix(proj, packed_all, params, maps)
    return finish(attend, scan, attend_out_weight, scan_out_weight)[None]


def solution(mesh):
    split = Mesh(
        mesh.devices.reshape(NZ, NY, mesh.shape["fs"], mesh.shape["tp"]),
        ("sp_0", "sp_1", "fs", "tp"),
    )
    in_specs = (
        P("fs", SP_TP, None),
        P(),
        P("fs", "tp"),
        P("fs", "tp"),
        P("fs", "tp"),
        P("fs", "tp"),
        P("tp", "fs", SP),
        P("tp"),
        P("tp", None),
        P("tp", None),
        P(None, "tp", None, None),
        P(None, "tp", None, None),
        P("tp"),
        P("tp", "fs", SP),
        P(None, "fs", "tp", None),
        P("tp", "fs"),
        P("tp", "fs"),
    )
    return jax.shard_map(
        on_device, mesh=split, in_specs=in_specs, out_specs=P("fs", SP_TP, None), check_vma=False
    )
```

time: 311 us -> 115 us (0.37)
  the two profiles are of different devices: /device:TPU:1 before, /device:TPU:225 now
where the time goes in v1:
time: 115 us
  Pallas kernels  110 us (96%)
  local copies, waits for them, and re-layouts  4.2 us (4%)
    pallas_call x1, Pallas kernels, mix(): pl.pallas_call(mix_kernel, out_shape=(jax.ShapeDtypeStruct((NY, 128, 128)...  43.2 us
    pallas_call x1, Pallas kernels, project(): pl.pallas_call(project_kernel, out_shape=(jax.ShapeDtypeStruct((4, NY, 12...  37.6 us
    pallas_call x1, Pallas kernels, finish(): pl.pallas_call(finish_kernel, out_shape=jax.ShapeDtypeStruct((64, 2048),...  28.9 us
    unnamed x34, local copies, waits for them, and re-layouts  2.93 us

profile of v1, /device:TPU:225, one launch (start us, length us, event | category | flops | bytes accessed | tf_op | source)
XLA Modules:
  0.0 114.7 jit_solution(10241769132722718918)
XLA Ops:
  0.0 1.1 slice_bitcast_fusion.1
  1.1 0.0 copy-start.8
  1.1 0.1 pad_maximum_fusion
  1.2 0.9 copy-done.8
  2.1 0.0 copy-start.13
  2.1 0.0 copy-start.14
  2.1 0.0 copy-start.10
  2.2 0.0 copy-start.5
  2.2 0.0 copy-start.6
  2.2 0.0 copy-start.2
  2.2 0.0 copy-start.3
  2.3 0.0 copy-start.4
  2.3 0.1 maximum_maximum_fusion.maps
  2.4 0.5 copy-done.9
  2.9 0.1 fusion
  3.0 0.1 fusion.1
  3.0 0.1 stack_broadcast_in_dim.12
  3.1 0.1 constant_dynamic-update-slice_fusion.1
  3.2 0.1 maximum_dynamic-update-slice_fusion
  3.3 0.0 copy-done.14
  3.3 0.1 pad.13.clone
  3.4 0.1 maximum_maximum_fusion.1.packed
  3.5 0.0 copy-done.2
  3.5 0.2 copy-done.3
  3.7 0.2 copy-done.4
  3.8 0.4 copy-done.7
  4.2 37.6 %project.1 = (bf16[4,4,128,128]{3,2,1,0:T(8,128)(2,1)S(1)}, f32[4,16,128]{2,1,0:T(8,128)S(1)}) custom-call(bf16[64,2048]{1,0:T(8,128)(2,1)S(1)} %bitcast.28, f32[1,2048]{1,0:T(1,128)S(1)} %bitcast.29, bf16[512,512]{1,0:T(8,128)(2,1)S(1)} %copy-done.2, bf16[512,512]{1,0:T(8,128)(2,1)S(1)} %copy-done.3, bf16[512,512]{1,0:T(8,128)(2,1)S(1)} %copy-done.4, ...), custom_call_target="tpu_custom_call" | custom-call | tf_op jit(solution)/shard_map/project/pallas_call | solution.py:131
  41.8 0.0 copy-start
  41.8 0.0 copy-start.1
  41.8 43.2 %mix.1 = (bf16[4,128,128]{2,1,0:T(8,128)(2,1)S(1)}, bf16[4,128,128]{2,1,0:T(8,128)(2,1)S(1)}) custom-call(bf16[4,4,128,128]{3,2,1,0:T(8,128)(2,1)S(1)} %get-tuple-element.9.proj, f32[4,16,128]{2,1,0:T(8,128)S(1)} %get-tuple-element.10.packed, f32[4,5,8,128]{3,2,1,0:T(8,128)S(1)} %constant_dynamic-update-slice_fusion.params, ...), custom_call_target="tpu_custom_call" | custom-call | tf_op jit(solution)/shard_map/mix/pallas_call | solution.py:419
  85.0 28.9 %finish.1 = bf16[64,2048]{1,0:T(8,128)(2,1)S(1)} custom-call(bf16[4,128,128]{2,1,0:T(8,128)(2,1)S(1)} %get-tuple-element.11.attend, bf16[4,128,128]{2,1,0:T(8,128)(2,1)S(1)} %get-tuple-element.12.scan, bf16[512,512]{1,0:T(8,128)(2,1)S(1)} %copy-done, bf16[512,512]{1,0:T(8,128)(2,1)S(1)} %copy-done.1), custom_call_target="tpu_custom_call" | custom-call | tf_op jit(solution)/shard_map/finish/pallas_call | solution.py:530
  114.0 0.7 copy.25
  (20 shorter events, 0.1 us)
Async XLA Ops:
  1.1 1.0 copy-start.8
  2.1 0.8 copy-start.9
  2.1 0.8 copy-start.11
  2.1 0.8 copy-start.12
  2.1 0.9 copy-start.15
  2.1 1.1 copy-start.13
  2.1 1.1 copy-start.14
  2.1 1.2 %copy-start.10 = (f32[32,1,128]{2,1,0:T(1,128)S(1)}, f32[32,1,128]{2,1,0:T(1,128)}, u32[]{:S(2)}) copy-start(f32[32,1,128]{2,1,0:T(1,128)} %param.30) | copy-start | bytes 49156
  2.2 1.3 %copy-start.5 = (bf16[512,512]{1,0:T(8,128)(2,1)S(1)}, bf16[512,512]{1,0:T(8,128)(2,1)}, u32[]{:S(2)}) copy-start(bf16[512,512]{1,0:T(8,128)(2,1)} %w_value.1) | copy-start | bytes 1572868
  2.2 1.3 %copy-start.6 = (bf16[1,64,2048]{2,1,0:T(8,128)(2,1)S(1)}, bf16[1,64,2048]{2,1,0:T(8,128)(2,1)}, u32[]{:S(2)}) copy-start(bf16[1,64,2048]{2,1,0:T(8,128)(2,1)} %param.17) | copy-start | bytes 786436
  2.2 1.3 %copy-start.2 = (bf16[512,512]{1,0:T(8,128)(2,1)S(1)}, bf16[512,512]{1,0:T(8,128)(2,1)}, u32[]{:S(2)}) copy-start(bf16[512,512]{1,0:T(8,128)(2,1)} %w_drive.1) | copy-start | bytes 1572868
  2.2 1.4 %copy-start.3 = (bf16[512,512]{1,0:T(8,128)(2,1)S(1)}, bf16[512,512]{1,0:T(8,128)(2,1)}, u32[]{:S(2)}) copy-start(bf16[512,512]{1,0:T(8,128)(2,1)} %w_query.1) | copy-start | bytes 1572868
  2.3 1.6 %copy-start.4 = (bf16[512,512]{1,0:T(8,128)(2,1)S(1)}, bf16[512,512]{1,0:T(8,128)(2,1)}, u32[]{:S(2)}) copy-start(bf16[512,512]{1,0:T(8,128)(2,1)} %w_key.1) | copy-start | bytes 1572868
  3.4 0.8 copy-start.7
  41.8 43.2 %copy-start = (bf16[512,512]{1,0:T(8,128)(2,1)S(1)}, bf16[512,512]{1,0:T(8,128)(2,1)}, u32[]{:S(2)}) copy-start(bf16[512,512]{1,0:T(8,128)(2,1)} %w_attend.1) | copy-start | bytes 1572868
  41.8 43.2 %copy-start.1 = (bf16[512,512]{1,0:T(8,128)(2,1)S(1)}, bf16[512,512]{1,0:T(8,128)(2,1)}, u32[]{:S(2)}) copy-start(bf16[512,512]{1,0:T(8,128)(2,1)} %w_scan.1) | copy-start | bytes 1572868

commit v2 on v1

v2 whole, which is shorter than its diff:
```python
import math

import jax
import jax.numpy as jnp
from jax import lax
from jax.experimental import pallas as pl
from jax.experimental.pallas import tpu as pltpu
from jax.sharding import Mesh
from jax.sharding import PartitionSpec as P

SP_TP = ("sp_0", "sp_1", "tp")
SP = ("sp_0", "sp_1")
EPSILON = 1e-06
LOG2E = 1.4426950408889634
NZ, NY, NX, NT = 8, 4, 4, 2
BF16, F32 = jnp.bfloat16, jnp.float32
VMEM = pl.BlockSpec(memory_space=pltpu.VMEM)
MESH_ID = pl.DeviceIdType.MESH


def remote(src, dst, send_sem, recv_sem, where):
    return pltpu.make_async_remote_copy(
        src_ref=src, dst_ref=dst, send_sem=send_sem, recv_sem=recv_sem,
        device_id=where, device_id_type=MESH_ID,
    )


def greet(peers):
    barrier = pltpu.get_barrier_semaphore()
    for peer in peers:
        pl.semaphore_signal(barrier, inc=1, device_id=peer, device_id_type=MESH_ID)


def await_greetings(count):
    pl.semaphore_wait(pltpu.get_barrier_semaphore(), count)


def plane_peers(x, y, t):
    peers = [
        {"fs": (x + dx) % NX, "tp": (t + dt) % NT}
        for dx in range(NX) for dt in range(NT) if (dx, dt) != (0, 0)
    ]
    peers += [
        {"fs": (x + dx) % NX, "sp_1": (y + dy) % NY} for dx in range(NX) for dy in range(1, NY)
    ]
    return peers


def high_low(value):
    high = value.astype(BF16)
    return high, (value - high.astype(F32)).astype(BF16)


def attend_pair(query, key, value, offset, fallen, ladder, visible):
    score = lax.dot_general(query, key, (((1,), (1,)), ((), ())), preferred_element_type=F32)
    score = score * (LOG2E * 128**-0.5) + offset
    soft = jnp.maximum(score, 0.0) + LOG2E * jnp.log(1.0 + jnp.exp2(-jnp.abs(score)))
    if visible is not None:
        soft = jnp.where(visible, soft, 0.0)
    sums = jnp.dot(
        jnp.concatenate(high_low(soft), axis=1), ladder, preferred_element_type=F32
    )
    behind = sums[:, :128] if fallen is None else sums[:, :128] + fallen
    weight = jnp.exp2(score + behind)
    if visible is not None:
        weight = jnp.where(visible, weight, 0.0)
    portion = jnp.dot(weight.astype(BF16), value, preferred_element_type=F32)
    total = sums[:, 128:] if fallen is None else sums[:, 128:] + fallen
    return portion, total


def turned(gain, state):
    return gain[0] * state + gain[1] * pltpu.roll(state, 64, 1)


def powers_times(left, right):
    return (
        left[0] * right[0] - left[1] * right[1],
        left[1] * right[0] + left[0] * right[1],
    )


def layer_kernel(
    tok, gain_ref, w_drive, w_query, w_key, w_value, packed, params, maps, w_attend, w_scan,
    out,
    normed, rows_in, keyed_w, query_w, drive_w, packed_in, driven_in, queries,
    own_in, right_in, left_in, far_in, offset_own, offset_in, state_own, state_in, acc, tot,
    ladder, into_map, out_map, fwd_p, fwd_q, inv_p, inv_q, held, ends, decay,
    attend_own, scan_own, attend_in, scan_in, part_out, part_in,
    s_rows, r_rows, s_half, r_half, s_weight, r_weight, s_packed, r_packed,
    s_right, r_right, s_left, r_left, s_offset, r_offset, s_state, r_state,
    s_attend, r_attend, s_scan, r_scan, s_part, r_part,
):
    z, y, x, t = (lax.axis_index(a) for a in ("sp_0", "sp_1", "fs", "tp"))
    greet(plane_peers(x, y, t) + [{"sp_0": (z + dz) % NZ} for dz in range(1, NZ)])
    row = lax.broadcasted_iota(jnp.int32, (128, 128), 0)
    lane = lax.broadcasted_iota(jnp.int32, (128, 128), 1)
    up, down = {"sp_0": (z + 1) % NZ}, {"sp_0": (z + NZ - 1) % NZ}
    sent = []

    def send(copy):
        copy.start()
        sent.append(copy)
        return copy

    values = tok[...].astype(F32)
    scale = lax.rsqrt(jnp.mean(values * values, axis=1, keepdims=True) + EPSILON)
    normed[...] = (values * scale * gain_ref[...]).astype(BF16)
    await_greetings(26)

    order = (0, 1, 3, 2)
    mine = pl.ds(pl.multiple_of(t * 64, 64), 64)
    sibling = {"tp": 1 - t}

    def row_copy(j):
        return remote(
            normed, rows_in.at[j, mine], s_rows.at[j], r_rows.at[j],
            {"sp_1": (y + order[j]) % NY},
        )

    def half_copy(j):
        return remote(
            rows_in.at[j, mine] if j else normed, rows_in.at[j, mine], s_half.at[j], r_half.at[j],
            sibling,
        )

    column = pl.ds(pl.multiple_of(y * 128, 128), 128)
    depth = pl.ds(pl.multiple_of(x * 512, 512), 512)
    sources = (w_key, w_value, w_query, w_drive)
    targets = (
        keyed_w.at[depth, :128], keyed_w.at[depth, 128:], query_w.at[depth], drive_w.at[depth]
    )

    def weight_copy(kind, dx):
        return remote(
            sources[kind].at[:, column], targets[kind], s_weight.at[kind, dx],
            r_weight.at[kind, dx], {"fs": (x + dx) % NX},
        )

    send(half_copy(0))
    for j in (1, 2, 3):
        send(row_copy(j))
    for kind in range(4):
        for dx in (1, 3, 2):
            send(weight_copy(kind, dx))
    packed_copies = [
        send(
            remote(
                packed.at[(y + dy) % NY], packed_in.at[y], s_packed.at[dy], r_packed.at[dy],
                {"sp_1": (y + dy) % NY},
            )
        )
        for dy in range(1, NY)
    ]
    packed_in[y] = packed[y]
    rows_in[0, mine] = normed[...]
    keyed_w[depth, :128] = w_key[:, column]
    keyed_w[depth, 128:] = w_value[:, column]
    query_w[depth] = w_query[:, column]
    drive_w[depth] = w_drive[:, column]

    sign = jnp.where(lane[:8] < 64, -1.0, 1.0)
    lam_real, lam_imag, log_step, initial, skip = (params[y, k] for k in range(5))
    step = jnp.exp(log_step)
    log_gain, rotate = lam_real * step, lam_imag * step
    cosine, sine, magnitude = jnp.cos(rotate), jnp.sin(rotate), jnp.exp(log_gain)
    bar_real, bar_imag = magnitude * cosine, magnitude * sine
    divisor = lam_real * lam_real + lam_imag * lam_imag
    shifted = bar_real - 1.0
    factor_real = (shifted * lam_real + bar_imag * lam_imag) / divisor
    factor_imag = (bar_imag * lam_real - shifted * lam_imag) / divisor * sign
    shrink = jnp.exp(-log_gain)
    gain = (bar_real, sign * bar_imag)
    inverse = (shrink * cosine, -sign * shrink * sine)
    gains, inverses = [gain], [inverse]
    for _ in range(9):
        gains.append(powers_times(gains[-1], gains[-1]))
    for _ in range(6):
        inverses.append(powers_times(inverses[-1], inverses[-1]))
    gain_block, gain_all = gains[7], gains[9]
    gain_last = powers_times(gain_block, inverse)
    into_map[...] = jnp.zeros_like(into_map)
    out_map[...] = jnp.zeros_like(out_map)
    for g in range(8):
        cols, swapped = pl.ds(g * 128, 128), pl.ds(1024 + g * 128, 128)
        raw = maps[y, 0, g]
        entry = factor_real[g : g + 1] * raw + factor_imag[g : g + 1] * pltpu.roll(raw, 64, 1)
        turned_entry = pltpu.roll(entry, 64, 1)
        for at in (g * 16, 128 + g * 16):
            into_map[at : at + 16, cols] = entry.astype(BF16)
            into_map[at : at + 16, swapped] = turned_entry.astype(BF16)
        raw = maps[y, 1, g]
        out_map[g * 16 : g * 16 + 16, cols] = (raw * -sign[:1]).astype(BF16)
        out_map[g * 16 : g * 16 + 16, swapped] = (pltpu.roll(raw, 64, 1) * -sign[:1]).astype(BF16)
        for table_p, table_q, steps in ((fwd_p, fwd_q, gains), (inv_p, inv_q, inverses)):
            real, imag = jnp.ones((8, 128), F32), jnp.zeros((8, 128), F32)
            for bit in range(3):
                by = tuple(part[g : g + 1] for part in steps[bit])
                new = powers_times((real, imag), by)
                chosen = (row[:8] & (1 << bit)) != 0
                real, imag = jnp.where(chosen, new[0], real), jnp.where(chosen, new[1], imag)
            table_p[:8, cols] = real
            table_q[:8, cols] = imag
            for bit in range(3, 7):
                n = 1 << bit
                by = tuple(part[g : g + 1] for part in steps[bit])
                new = powers_times((table_p[:n, cols], table_q[:n, cols]), by)
                table_p[n : 2 * n, cols] = new[0]
                table_q[n : 2 * n, cols] = new[1]
    ladder_row = lax.broadcasted_iota(jnp.int32, (256, 256), 0) % 128
    ladder_lane = lax.broadcasted_iota(jnp.int32, (256, 256), 1)
    ladder[...] = jnp.where((ladder_lane >= 128) | (ladder_row >= ladder_lane), -1.0, 0.0).astype(
        BF16
    )

    def block_of(j):
        dy = j + j // 2 * (5 - 2 * j)
        return (y + NY - dy) % NY

    def right_copy(i, j):
        b = block_of(j)
        return remote(
            own_in.at[b] if i == 1 else right_in.at[i - 2, b],
            far_in.at[b] if i == 4 else right_in.at[i - 1, b],
            s_right.at[i - 1, j], r_right.at[i - 1, j], up,
        )

    def left_copy(i, j):
        b = block_of(j)
        return remote(
            own_in.at[b] if i == 1 else left_in.at[i - 2, b],
            far_in.at[b] if i == 4 else left_in.at[i - 1, b],
            s_left.at[i - 1, j], r_left.at[i - 1, j], down,
        )

    def own_keys(first, last):
        product = jnp.dot(
            rows_in[first:last].reshape((last - first) * 128, 2048), keyed_w[...],
            preferred_element_type=F32,
        ).astype(BF16)
        for j in range(first, last):
            own_in[block_of(j)] = product[(j - first) * 128 : (j - first + 1) * 128]
            right_copy(1, j).start()
            left_copy(1, j).start()

    for j in (1, 2):
        row_copy(j).wait_recv()
        send(half_copy(j))
    for copy in packed_copies:
        copy.wait_recv()
    for b in range(NY):
        offset_own[b : b + 1, :] = packed_in[b, 8:9, :]
        offset_in[0, b : b + 1, :] = packed_in[b, 8:9, :]
    offset_own[4:8, :] = jnp.zeros((4, 128), F32)
    offset_copies = [
        send(
            remote(
                offset_own, offset_in.at[dz], s_offset.at[dz], r_offset.at[dz],
                {"sp_0": (z + dz) % NZ},
            )
        )
        for dz in range(1, NZ)
    ]
    for kind in (0, 1):
        for dx in (1, 3, 2):
            weight_copy(kind, dx).wait_recv()
    for j in (0, 1, 2):
        half_copy(j).wait_recv()
    own_keys(0, 3)
    row_copy(3).wait_recv()
    send(half_copy(3))
    half_copy(3).wait_recv()
    own_keys(3, 4)
    until = jnp.where(lane <= row, 1.0, 0.0)
    until_half = until.astype(BF16)
    falls = []
    for b in range(NY):
        forget = packed_in[b, :8, :]
        spread = jnp.concatenate(
            [jnp.broadcast_to(forget[g : g + 1], (16, 128)) for g in range(8)], axis=0
        )
        decay[b] = lax.dot_general(
            until, spread, (((1,), (1,)), ((), ())), preferred_element_type=F32,
            precision=lax.Precision.HIGHEST,
        )
        falls.append(jnp.sum(forget, axis=1, keepdims=True))
    for dx in (1, 3, 2):
        weight_copy(2, dx).wait_recv()
    product = jnp.dot(
        rows_in[...].reshape(512, 2048), query_w[...], preferred_element_type=F32
    ).astype(BF16)
    for j in range(NY):
        queries[block_of(j)] = product[j * 128 : (j + 1) * 128]

    def arrive(i, j):
        right_copy(i, j).wait_recv()
        left_copy(i, j).wait_recv()
        if i < 3:
            right_copy(i + 1, j).start()
            left_copy(i + 1, j).start()
            return

        @pl.when(j < 2)
        def _():
            right_copy(4, j).start()

        @pl.when(j >= 2)
        def _():
            left_copy(4, j).start()

    for j in range(NY):
        arrive(1, j)

    for q in range(NY):
        portion_sum, fallen = None, None
        for k in range(q, -1, -1):
            portion, fallen = attend_pair(
                queries[q], own_in[k, :, :128], own_in[k, :, 128:], offset_in[0, k : k + 1, :],
                fallen, ladder[...], lane < row if k == q else None,
            )
            portion_sum = portion if portion_sum is None else portion_sum + portion
        acc[0, q] = portion_sum
        tot[0, q] = fallen
    for copy in offset_copies:
        copy.wait_recv()

    for dx in (1, 3, 2):
        weight_copy(3, dx).wait_recv()
    product = jnp.dot(
        rows_in[...].reshape(512, 2048), drive_w[...], preferred_element_type=F32
    ).astype(BF16)
    for j in range(NY):
        driven_in[block_of(j)] = product[j * 128 : (j + 1) * 128]
    local = jnp.zeros((8, 128), F32)
    fall_all = jnp.zeros((8, 1), F32)
    for b in range(NY):
        driven = driven_in[b].astype(F32) * jnp.exp(-decay[b])
        entered = jnp.dot(
            jnp.concatenate(high_low(driven), axis=1), into_map[...], preferred_element_type=F32
        )
        unturned = entered[:, :1024] * inv_p[...] + entered[:, 1024:] * inv_q[...]
        high, low = high_low(unturned)
        held[b] = jnp.dot(until_half, high, preferred_element_type=F32) + jnp.dot(
            until_half, low, preferred_element_type=F32
        )
        for g in range(8):
            ends[b, g : g + 1, :] = held[b, 127:128, g * 128 : (g + 1) * 128]
        fall_all = fall_all + falls[b]
        falls[b] = jnp.exp(falls[b])
        ends[b] = falls[b] * turned(gain_last, ends[b])
        local = falls[b] * turned(gain_block, local) + ends[b]
        arrive(2, b)
    state_own[:8, :] = local
    state_own[8:, :] = jnp.broadcast_to(fall_all, (8, 128))
    state_copies = [
        send(
            remote(
                state_own, state_in.at[dz], s_state.at[dz], r_state.at[dz],
                {"sp_0": (z + dz) % NZ},
            )
        )
        for dz in range(1, NZ)
    ]

    def attend_block(dz, pairs, k):
        offset = offset_in[dz, pl.ds(k, 1), :]
        for q in range(NY):
            portion, fallen = attend_pair(
                queries[q], pairs[k, :, :128], pairs[k, :, 128:], offset, tot[dz, q],
                ladder[...], None,
            )
            acc[dz, q] += portion
            tot[dz, q] = fallen

    def attend_step(i):
        chunks = [(i, right_in.at[i - 1]), (8 - i, left_in.at[i - 1])] if i < 4 else [(4, far_in)]
        for dz, _ in chunks:
            @pl.when(z >= dz)
            def _():
                acc[dz] = jnp.zeros((NY, 128, 128), F32)
                tot[dz] = jnp.zeros((NY, 128, 128), F32)

        def one(turn, carry):
            if i < 2:
                arrive(i + 2, turn)
            elif i == 2:
                @pl.when(turn < 2)
                def _():
                    right_copy(4, turn).wait_recv()

                @pl.when(turn >= 2)
                def _():
                    left_copy(4, turn).wait_recv()

            for dz, pairs in chunks:
                @pl.when(z >= dz)
                def _():
                    attend_block(dz, pairs, NY - 1 - turn)

            return carry

        lax.fori_loop(0, NY, one, 0)

    attend_step(1)
    attend_step(2)

    for copy in state_copies:
        copy.wait_recv()
    carry = initial
    for source in range(NZ - 1):
        arrived = state_in[jnp.maximum(z - source, 1)]
        moved = jnp.exp(arrived[8:]) * turned(gain_all, carry) + arrived[:8]
        carry = jnp.where(source < z, moved, carry)
    for b in range(NY):
        entering = turned(gain, carry)
        whole = jnp.concatenate(
            [held[b, :, g * 128 : (g + 1) * 128] + entering[g : g + 1] for g in range(8)], axis=1
        )
        turned_states = jnp.concatenate(
            [(whole * fwd_p[...]).astype(BF16), (whole * fwd_q[...]).astype(BF16)], axis=1
        )
        read = lax.dot_general(
            turned_states, out_map[...], (((1,), (1,)), ((), ())), preferred_element_type=F32
        )
        read = read * jnp.exp(decay[b]) + skip[:1] * driven_in[b].astype(F32)
        inner = math.sqrt(2.0 / math.pi) * (read + 0.044715 * (read * read * read))
        scan_own[b] = (0.5 * read * (1.0 + jnp.tanh(inner))).astype(BF16)
        carry = falls[b] * turned(gain_block, carry) + ends[b]

    def spread_copies(own, landing, s_sem, r_sem):
        return {
            (dx, dy): remote(
                own.at[(y + dy) % NY], landing.at[dx, dy], s_sem.at[dx, dy], r_sem.at[dx, dy],
                {"fs": (x + dx) % NX, "sp_1": (y + dy) % NY},
            )
            for dx in order for dy in (1, 3, 2, 0) if (dx, dy) != (0, 0)
        }

    scan_copies = spread_copies(scan_own, scan_in, s_scan, r_scan)
    for copy in scan_copies.values():
        send(copy)
    scan_in[0, 0] = scan_own[y]
    attend_step(3)
    attend_step(4)
    for dz in range(1, NZ):
        @pl.when(z >= dz)
        def _():
            for q in range(NY):
                fallen = tot[0, q]
                acc[0, q] += jnp.exp2(fallen) * acc[dz, q]
                tot[0, q] = fallen + tot[dz, q]

    for q in range(NY):
        attend_own[q] = acc[0, q].astype(BF16)
    attend_copies = spread_copies(attend_own, attend_in, s_attend, r_attend)
    for copy in attend_copies.values():
        send(copy)
    attend_in[0, 0] = attend_own[y]

    part_copies = {}
    for dx in order:
        total = None
        for dy in range(NY):
            if (dx, dy) != (0, 0):
                scan_copies[dx, dy].wait_recv()
                attend_copies[dx, dy].wait_recv()
            head = (y + NY - dy) % NY
            head_rows = pl.ds(pl.multiple_of(head * 128, 128), 128)
            product = jnp.dot(
                attend_in[dx, dy], w_attend[head_rows, :], preferred_element_type=F32
            ) + jnp.dot(scan_in[dx, dy], w_scan[head_rows, :], preferred_element_type=F32)
            total = product if total is None else total + product
        rounded = total.astype(BF16)
        for k in range(NT):
            part_out[dx, k] = rounded[k * 64 : (k + 1) * 64]
        for dt in range(NT):
            if (dx, dt) != (0, 0):
                to = (t + dt) % NT
                part_copies[dx, dt] = send(
                    remote(
                        part_out.at[dx, to], part_in.at[dx, dt], s_part.at[dx, dt],
                        r_part.at[dx, dt], {"fs": (x + NX - dx) % NX, "tp": to},
                    )
                )
    part_in[0, 0] = part_out[0, t]
    for dx in order:
        for dt in range(NT):
            if (dx, dt) != (0, 0):
                part_copies[dx, dt].wait_recv()
        columns = pl.ds(pl.multiple_of((x + dx) % NX * 512, 512), 512)
        out[:, columns] = (part_in[dx, 0].astype(F32) + part_in[dx, 1].astype(F32)).astype(BF16)
    for copy in sent:
        copy.wait_send()
    for i in range(1, 5):
        for j in range(NY):
            if i < 4 or j < 2:
                right_copy(i, j).wait_send()
            if i < 4 or j >= 2:
                left_copy(i, j).wait_send()


def layer(*operands):
    def sems(*shape):
        return [pltpu.SemaphoreType.DMA(shape)] * 2

    return pl.pallas_call(
        layer_kernel,
        out_shape=jax.ShapeDtypeStruct((64, 2048), BF16),
        in_specs=[VMEM] * 11,
        out_specs=VMEM,
        scratch_shapes=[
            pltpu.VMEM((64, 2048), BF16),
            pltpu.VMEM((NY, 128, 2048), BF16),
            pltpu.VMEM((2048, 256), BF16),
            pltpu.VMEM((2048, 128), BF16),
            pltpu.VMEM((2048, 128), BF16),
            pltpu.VMEM((NY, 16, 128), F32),
            pltpu.VMEM((NY, 128, 128), BF16),
            pltpu.VMEM((NY, 128, 128), BF16),
            pltpu.VMEM((NY, 128, 256), BF16),
            pltpu.VMEM((3, NY, 128, 256), BF16),
            pltpu.VMEM((3, NY, 128, 256), BF16),
            pltpu.VMEM((NY, 128, 256), BF16),
            pltpu.VMEM((8, 128), F32),
            pltpu.VMEM((NZ, 8, 128), F32),
            pltpu.VMEM((16, 128), F32),
            pltpu.VMEM((NZ, 16, 128), F32),
            pltpu.VMEM((NZ, NY, 128, 128), F32),
            pltpu.VMEM((NZ, NY, 128, 128), F32),
            pltpu.VMEM((256, 256), BF16),
            pltpu.VMEM((256, 2048), BF16),
            pltpu.VMEM((128, 2048), BF16),
            pltpu.VMEM((128, 1024), F32),
            pltpu.VMEM((128, 1024), F32),
            pltpu.VMEM((128, 1024), F32),
            pltpu.VMEM((128, 1024), F32),
            pltpu.VMEM((NY, 128, 1024), F32),
            pltpu.VMEM((NY, 8, 128), F32),
            pltpu.VMEM((NY, 128, 128), F32),
            pltpu.VMEM((NY, 128, 128), BF16),
            pltpu.VMEM((NY, 128, 128), BF16),
            pltpu.VMEM((NX, NY, 128, 128), BF16),
            pltpu.VMEM((NX, NY, 128, 128), BF16),
            pltpu.VMEM((NX, NT, 64, 512), BF16),
            pltpu.VMEM((NX, NT, 64, 512), BF16),
            *sems(NY), *sems(NY), *sems(4, NX), *sems(NY), *sems(4, NY), *sems(4, NY), *sems(NZ),
            *sems(NZ), *sems(NX, NY), *sems(NX, NY), *sems(NX, NT),
        ],
        compiler_params=pltpu.CompilerParams(
            collective_id=0, has_side_effects=True, vmem_limit_bytes=56 << 20
        ),
        name="layer",
    )(*operands)


def on_device(
    tokens, norm_gain, drive_weight, query_weight, key_weight, value_weight, key_offset, log_step,
    lambda_real, lambda_imag, input_map, output_map, skip_gain, forget, initial_state,
    scan_out_weight, attend_out_weight,
):
    packed = jnp.concatenate(
        [
            forget[:, 0, :].reshape(NY, 8, 128),
            (key_offset[:, 0, :].astype(F32) * LOG2E).reshape(NY, 1, 128),
            jnp.zeros((NY, 7, 128), F32),
        ],
        axis=1,
    )

    def twice(array):
        return jnp.concatenate([array, array], axis=-1).reshape(NY, 8, 128)

    params = jnp.stack(
        [
            twice(lambda_real),
            twice(lambda_imag),
            jnp.broadcast_to(log_step.reshape(NY, 8, 1), (NY, 8, 128)),
            jnp.concatenate([initial_state[0, 0], initial_state[1, 0]], axis=-1).reshape(
                NY, 8, 128
            ),
            jnp.broadcast_to(skip_gain.reshape(NY, 1, 128), (NY, 8, 128)),
        ],
        axis=1,
    )
    maps = jnp.stack(
        [
            jnp.concatenate([input_map[0], input_map[1]], axis=1)
            .transpose(0, 2, 1)
            .reshape(NY, 8, 16, 128),
            jnp.concatenate([output_map[0], output_map[1]], axis=2).reshape(NY, 8, 16, 128),
        ],
        axis=1,
    )
    weights = (drive_weight, query_weight, key_weight, value_weight)
    return layer(
        tokens[0], norm_gain[None], *weights, packed, params, maps, attend_out_weight,
        scan_out_weight,
    )[None]


def solution(mesh):
    split = Mesh(
        mesh.devices.reshape(NZ, NY, mesh.shape["fs"], mesh.shape["tp"]),
        ("sp_0", "sp_1", "fs", "tp"),
    )
    in_specs = (
        P("fs", SP_TP, None),
        P(),
        P("fs", "tp"),
        P("fs", "tp"),
        P("fs", "tp"),
        P("fs", "tp"),
        P("tp", "fs", SP),
        P("tp"),
        P("tp", None),
        P("tp", None),
        P(None, "tp", None, None),
        P(None, "tp", None, None),
        P("tp"),
        P("tp", "fs", SP),
        P(None, "fs", "tp", None),
        P("tp", "fs"),
        P("tp", "fs"),
    )
    return jax.shard_map(
        on_device, mesh=split, in_specs=in_specs, out_specs=P("fs", SP_TP, None), check_vma=False
    )
```

time: 115 us -> 95.5 us (0.83)
  Pallas kernels: 110 us -> 86 us
  local copies, waits for them, and re-layouts: 4.2 us -> 7.13 us
  other arithmetic: 0.58 us -> 1.99 us
    pallas_call x3 -> x1, Pallas kernels: 110 us -> 86 us  [layer(): pl.pallas_call(layer_kernel, out_shape=jax.ShapeDtypeStruct((64, 2048), B...]
    unnamed x34 -> x20, local copies, waits for them, and re-layouts: 2.93 us -> 5.87 us
where the time goes in v2:
time: 95.5 us; the launch traced here: 95.1 us
  Pallas kernels  86 us (90%)
  local copies, waits for them, and re-layouts  7.13 us (7%)
  other arithmetic  1.99 us (2%)
    pallas_call x1, Pallas kernels, layer(): pl.pallas_call(layer_kernel, out_shape=jax.ShapeDtypeStruct((64, 2048), B...  86 us
    unnamed x20, local copies, waits for them, and re-layouts  5.87 us

profile of v2, /device:TPU:225, one launch (start us, length us, event | category | flops | bytes accessed | tf_op | source)
XLA Modules:
  0.0 95.1 jit_solution(15098398348399675785)
XLA Ops:
  0.0 1.1 %slice_bitcast_fusion.1 = (f32[32,64,16]{1,2,0:T(8,128)S(1)}, f32[32,64,16]{1,2,0:T(8,128)S(1)}) fusion(f32[2,32,64,16]{2,3,1,0:T(8,128)} %param.27), kind=kLoop, calls=%fused_computation.3 | loop fusion | bytes 524288 | tf_op jit(solution)/shard_map/squeeze | solution.py:587
  1.1 0.0 copy-start
  1.1 0.1 pad_maximum_fusion
  1.2 0.9 copy-done
  2.1 0.0 copy-start.2
  2.2 0.9 maximum_maximum_fusion.maps
  3.1 0.0 copy-done.2
  3.1 0.0 copy-start.4
  3.1 0.7 copy-done.4
  3.8 0.0 copy-start.5
  3.8 0.1 fusion
  3.9 0.6 copy-done.5
  4.5 0.0 copy-start.8
  4.5 0.1 fusion.1
  4.6 0.6 copy-done.8
  5.2 0.1 stack_broadcast_in_dim.12
  5.3 0.1 constant_dynamic-update-slice_fusion.1
  5.3 0.0 copy-start.6
  5.3 0.1 maximum_dynamic-update-slice_fusion
  5.4 0.6 copy-done.6
  6.0 0.0 copy-start.7
  6.0 0.0 copy-start.3
  6.0 0.7 copy-done.7
  6.7 0.0 copy-start.1
  6.7 0.1 pad.13.clone
  6.8 0.0 copy-done.3
  6.8 0.7 maximum_maximum_fusion.1.packed
  7.5 0.0 copy-done.1
  7.5 86.0 %layer.1 = bf16[64,2048]{1,0:T(8,128)(2,1)} custom-call(bf16[64,2048]{1,0:T(8,128)(2,1)} %bitcast.31, f32[1,2048]{1,0:T(1,128)} %bitcast.33, bf16[512,512]{1,0:T(8,128)(2,1)} %w_drive.1, bf16[512,512]{1,0:T(8,128)(2,1)} %w_query.1, bf16[512,512]{1,0:T(8,128)(2,1)} %w_key.1, bf16[512,512]{1,0:T(8,128)(2,1)} %w_value.1, ...), custom_call_target="tpu_custom_call" | custom-call | tf_op jit(solution)/shard_map/layer/pallas_call | solution.py:506
  93.5 1.7 %copy.25 = bf16[1,64,2048]{2,1,0:T(8,128)(2,1)} copy(bf16[1,64,2048]{2,1,0:T(8,128)(2,1)} %bitcast.28) | data formatting | bytes 524288
  (6 shorter events, 0.1 us)
Async XLA Ops:
  1.1 1.0 %copy-start = (f32[2,32,16,64]{3,2,1,0:T(8,128)S(1)}, f32[2,32,16,64]{3,2,1,0:T(8,128)}, u32[]{:S(2)}) copy-start(f32[2,32,16,64]{3,2,1,0:T(8,128)} %param.28) | copy-start | bytes 786436
  2.1 0.9 copy-start.2
  3.1 0.7 copy-start.4
  3.8 0.7 copy-start.5
  4.5 0.7 copy-start.8
  5.3 0.7 copy-start.6
  6.0 0.7 copy-start.7
  6.0 0.8 copy-start.3
  6.7 0.8 copy-start.1

commit v3 on v2

--- a/solution.py
+++ b/solution.py
@@ -81,9 +81,15 @@
 
 
 def layer_kernel(
-    tok, gain_ref, w_drive, w_query, w_key, w_value, packed, params, maps, w_attend, w_scan,
-    out,
-    normed, rows_in, keyed_w, query_w, drive_w, packed_in, driven_in, queries,
+    *refs,
+):
+    operands, outs, held_here, rest = refs[:17], refs[17:19], refs[19:36], refs[36:]
+    run_layer(operands, outs, held_here, *rest)
+
+
+def run_layer(
+    operands, outs, held_here, s_operand,
+    normed, rows_in, keyed_w, query_w, drive_w, packed, packed_in, driven_in, queries,
     own_in, right_in, left_in, far_in, offset_own, offset_in, state_own, state_in, acc, tot,
     ladder, into_map, out_map, fwd_p, fwd_q, inv_p, inv_q, held, ends, decay,
     attend_own, scan_own, attend_in, scan_in, part_out, part_in,
@@ -91,6 +97,16 @@
     s_right, r_right, s_left, r_left, s_offset, r_offset, s_state, r_state,
     s_attend, r_attend, s_scan, r_scan, s_part, r_part,
 ):
+    (
+        tok, gain_ref, w_drive, w_query, w_key, w_value, key_offset, log_step_ref, lambda_real,
+        lambda_imag, input_map, output_map, skip_ref, forget_ref, initial_ref, w_attend, w_scan,
+    ) = held_here
+    fetches = [
+        pltpu.make_async_copy(src, dst, s_operand.at[k])
+        for k, (src, dst) in enumerate(zip(operands, held_here))
+    ]
+    for fetch in fetches:
+        fetch.start()
     z, y, x, t = (lax.axis_index(a) for a in ("sp_0", "sp_1", "fs", "tp"))
     greet(plane_peers(x, y, t) + [{"sp_0": (z + dz) % NZ} for dz in range(1, NZ)])
     row = lax.broadcasted_iota(jnp.int32, (128, 128), 0)
@@ -103,9 +119,18 @@
         sent.append(copy)
         return copy
 
+    for k in (0, 1, 6, 13):
+        fetches[k].wait()
+    packed[:, :8, :] = forget_ref[...]
+    packed[:, 8:, :] = jnp.zeros((NY, 8, 128), F32)
+    offsets = key_offset[...].astype(F32) * LOG2E
+    for k in range(NY):
+        packed[k, 8:9, :] = offsets[k : k + 1]
     values = tok[...].astype(F32)
     scale = lax.rsqrt(jnp.mean(values * values, axis=1, keepdims=True) + EPSILON)
     normed[...] = (values * scale * gain_ref[...]).astype(BF16)
+    for k in (2, 3, 4, 5):
+        fetches[k].wait()
     await_greetings(26)
 
     order = (0, 1, 3, 2)
@@ -159,9 +184,23 @@
     query_w[depth] = w_query[:, column]
     drive_w[depth] = w_drive[:, column]
 
+    for k in (7, 8, 9, 10, 11, 12, 14, 15, 16):
+        fetches[k].wait()
     sign = jnp.where(lane[:8] < 64, -1.0, 1.0)
-    lam_real, lam_imag, log_step, initial, skip = (params[y, k] for k in range(5))
-    step = jnp.exp(log_step)
+    groups = pl.ds(pl.multiple_of(y * 8, 8), 8)
+
+    def side_by_side(left, right):
+        return jnp.concatenate([left, right], axis=1)
+
+    lam_real = side_by_side(lambda_real[groups, :], lambda_real[groups, :])
+    lam_imag = side_by_side(lambda_imag[groups, :], lambda_imag[groups, :])
+    initial = side_by_side(initial_ref[0, groups, :], initial_ref[1, groups, :])
+    spot = lax.broadcasted_iota(jnp.int32, (8, 32), 1) - lax.broadcasted_iota(
+        jnp.int32, (8, 32), 0
+    )
+    step = jnp.exp(
+        jnp.sum(jnp.where(spot == y * 8, log_step_ref[...], 0.0), axis=1, keepdims=True)
+    )
     log_gain, rotate = lam_real * step, lam_imag * step
     cosine, sine, magnitude = jnp.cos(rotate), jnp.sin(rotate), jnp.exp(log_gain)
     bar_real, bar_imag = magnitude * cosine, magnitude * sine
@@ -183,13 +222,13 @@
     out_map[...] = jnp.zeros_like(out_map)
     for g in range(8):
         cols, swapped = pl.ds(g * 128, 128), pl.ds(1024 + g * 128, 128)
-        raw = maps[y, 0, g]
+        raw = side_by_side(input_map[0, y * 8 + g], input_map[1, y * 8 + g])
         entry = factor_real[g : g + 1] * raw + factor_imag[g : g + 1] * pltpu.roll(raw, 64, 1)
         turned_entry = pltpu.roll(entry, 64, 1)
         for at in (g * 16, 128 + g * 16):
             into_map[at : at + 16, cols] = entry.astype(BF16)
             into_map[at : at + 16, swapped] = turned_entry.astype(BF16)
-        raw = maps[y, 1, g]
+        raw = side_by_side(output_map[0, y * 8 + g], output_map[1, y * 8 + g])
         out_map[g * 16 : g * 16 + 16, cols] = (raw * -sign[:1]).astype(BF16)
         out_map[g * 16 : g * 16 + 16, swapped] = (pltpu.roll(raw, 64, 1) * -sign[:1]).astype(BF16)
         for table_p, table_q, steps in ((fwd_p, fwd_q, gains), (inv_p, inv_q, inverses)):
@@ -422,7 +461,7 @@
         read = lax.dot_general(
             turned_states, out_map[...], (((1,), (1,)), ((), ())), preferred_element_type=F32
         )
-        read = read * jnp.exp(decay[b]) + skip[:1] * driven_in[b].astype(F32)
+        read = read * jnp.exp(decay[b]) + skip_ref[pl.ds(y, 1), :] * driven_in[b].astype(F32)
         inner = math.sqrt(2.0 / math.pi) * (read + 0.044715 * (read * read * read))
         scan_own[b] = (0.5 * read * (1.0 + jnp.tanh(inner))).astype(BF16)
         carry = falls[b] * turned(gain_block, carry) + ends[b]
@@ -488,7 +527,8 @@
             if (dx, dt) != (0, 0):
                 part_copies[dx, dt].wait_recv()
         columns = pl.ds(pl.multiple_of((x + dx) % NX * 512, 512), 512)
-        out[:, columns] = (part_in[dx, 0].astype(F32) + part_in[dx, 1].astype(F32)).astype(BF16)
+        for dt in range(NT):
+            outs[dt][:, columns] = part_in[dx, dt]
     for copy in sent:
         copy.wait_send()
     for i in range(1, 5):
@@ -505,15 +545,18 @@
 
     return pl.pallas_call(
         layer_kernel,
-        out_shape=jax.ShapeDtypeStruct((64, 2048), BF16),
-        in_specs=[VMEM] * 11,
-        out_specs=VMEM,
+        out_shape=[jax.ShapeDtypeStruct((64, 2048), BF16)] * NT,
+        in_specs=[pl.BlockSpec(memory_space=pl.ANY)] * 17,
+        out_specs=[VMEM] * NT,
         scratch_shapes=[
+            *(pltpu.VMEM(operand.shape, operand.dtype) for operand in operands),
+            pltpu.SemaphoreType.DMA((17,)),
             pltpu.VMEM((64, 2048), BF16),
             pltpu.VMEM((NY, 128, 2048), BF16),
             pltpu.VMEM((2048, 256), BF16),
             pltpu.VMEM((2048, 128), BF16),
             pltpu.VMEM((2048, 128), BF16),
+            pltpu.VMEM((NY, 16, 128), F32),
             pltpu.VMEM((NY, 16, 128), F32),
             pltpu.VMEM((NY, 128, 128), BF16),
             pltpu.VMEM((NY, 128, 128), BF16),
@@ -547,7 +590,7 @@
             *sems(NZ), *sems(NX, NY), *sems(NX, NY), *sems(NX, NT),
         ],
         compiler_params=pltpu.CompilerParams(
-            collective_id=0, has_side_effects=True, vmem_limit_bytes=56 << 20
+            collective_id=0, has_side_effects=True, vmem_limit_bytes=60 << 20
         ),
         name="layer",
     )(*operands)
@@ -558,44 +601,26 @@
     lambda_real, lambda_imag, input_map, output_map, skip_gain, forget, initial_state,
     scan_out_weight, attend_out_weight,
 ):
-    packed = jnp.concatenate(
-        [
-            forget[:, 0, :].reshape(NY, 8, 128),
-            (key_offset[:, 0, :].astype(F32) * LOG2E).reshape(NY, 1, 128),
-            jnp.zeros((NY, 7, 128), F32),
-        ],
-        axis=1,
-    )
-
-    def twice(array):
-        return jnp.concatenate([array, array], axis=-1).reshape(NY, 8, 128)
-
-    params = jnp.stack(
-        [
-            twice(lambda_real),
-            twice(lambda_imag),
-            jnp.broadcast_to(log_step.reshape(NY, 8, 1), (NY, 8, 128)),
-            jnp.concatenate([initial_state[0, 0], initial_state[1, 0]], axis=-1).reshape(
-                NY, 8, 128
-            ),
-            jnp.broadcast_to(skip_gain.reshape(NY, 1, 128), (NY, 8, 128)),
-        ],
-        axis=1,
-    )
-    maps = jnp.stack(
-        [
-            jnp.concatenate([input_map[0], input_map[1]], axis=1)
-            .transpose(0, 2, 1)
-            .reshape(NY, 8, 16, 128),
-            jnp.concatenate([output_map[0], output_map[1]], axis=2).reshape(NY, 8, 16, 128),
-        ],
-        axis=1,
-    )
-    weights = (drive_weight, query_weight, key_weight, value_weight)
-    return layer(
-        tokens[0], norm_gain[None], *weights, packed, params, maps, attend_out_weight,
+    parts = layer(
+        tokens[0],
+        norm_gain[None],
+        drive_weight,
+        query_weight,
+        key_weight,
+        value_weight,
+        key_offset[:, 0, :],
+        log_step[None],
+        lambda_real,
+        lambda_imag,
+        input_map.transpose(0, 1, 3, 2),
+        output_map,
+        skip_gain.reshape(NY, 128),
+        forget.reshape(NY, 8, 128),
+        initial_state[:, 0],
+        attend_out_weight,
         scan_out_weight,
-    )[None]
+    )
+    return (parts[0].astype(F32) + parts[1].astype(F32)).astype(BF16)[None]
 
 
 def solution(mesh):

time: 95.5 us -> 86.1 us (0.902)
  local copies, waits for them, and re-layouts: 7.13 us -> 0 us
  Pallas kernels: 86 us -> 84.2 us
    unnamed x20 -> x0, local copies, waits for them, and re-layouts: 5.87 us -> none
    broadcast_in_dim x0 -> x1, other arithmetic: none -> 1.8 us  [on_device(): return (parts[0].astype(F32) + parts[1].astype(F32)).astype(BF16)[None]]
    pallas_call x1, Pallas kernels: 86 us -> 84.2 us  [layer(): pl.pallas_call(layer_kernel, out_shape=[jax.ShapeDtypeStruct((64, 2048),...]
    squeeze x1 -> x0, local copies, waits for them, and re-layouts: 1.06 us -> none  [on_device(): input_map[0]]
where the time goes in v3:
time: 86.1 us; the launch traced here: 86 us
  Pallas kernels  84.2 us (98%)
  other arithmetic  1.8 us (2%)
    pallas_call x1, Pallas kernels, layer(): pl.pallas_call(layer_kernel, out_shape=[jax.ShapeDtypeStruct((64, 2048),...  84.2 us
    broadcast_in_dim x1, other arithmetic, on_device(): return (parts[0].astype(F32) + parts[1].astype(F32)).astype(BF16)[None]  1.8 us

profile of v3, /device:TPU:225, one launch (start us, length us, event | category | flops | bytes accessed | tf_op | source)
XLA Modules:
  0.0 86.0 jit_solution(4599059246750221865)
XLA Ops:
  0.0 84.2 %layer.1 = (bf16[64,2048]{1,0:T(8,128)(2,1)}, bf16[64,2048]{1,0:T(8,128)(2,1)}) custom-call(bf16[64,2048]{1,0:T(8,128)(2,1)} %bitcast.11, f32[1,2048]{1,0:T(1,128)} %bitcast.14, bf16[512,512]{1,0:T(8,128)(2,1)} %refs_2_.1, bf16[512,512]{1,0:T(8,128)(2,1)} %refs_3_.1, bf16[512,512]{1,0:T(8,128)(2,1)} %refs_4_.1, bf16[512,512]{1,0:T(8,128)(2,1)} %refs_5_.1, ...), custom_call_target="tpu_custom_call" | custom-call | tf_op jit(solution)/shard_map/layer/pallas_call | solution.py:546
  84.3 1.8 %fusion = bf16[1,64,2048]{2,1,0:T(8,128)(2,1)} fusion(bf16[64,2048]{1,0:T(8,128)(2,1)} %get-tuple-element.8, bf16[64,2048]{1,0:T(8,128)(2,1)} %get-tuple-element.7), kind=kLoop, calls=%fused_computation.1 | loop fusion | flops 524288 | bytes 786432 | tf_op jit(solution)/shard_map/broadcast_in_dim | solution.py:623

commit v4 on v3

--- a/solution.py
+++ b/solution.py
@@ -51,22 +51,22 @@
     return high, (value - high.astype(F32)).astype(BF16)
 
 
-def attend_pair(query, key, value, offset, fallen, ladder, visible):
-    score = lax.dot_general(query, key, (((1,), (1,)), ((), ())), preferred_element_type=F32)
-    score = score * (LOG2E * 128**-0.5) + offset
-    soft = jnp.maximum(score, 0.0) + LOG2E * jnp.log(1.0 + jnp.exp2(-jnp.abs(score)))
+def attend_chunk(query, pairs, offset, ladder, visible=None):
+    keys, values = pairs[:, :128], pairs[:, 128:]
+    score = lax.dot_general(query, keys, (((1,), (1,)), ((), ())), preferred_element_type=F32)
+    score = score + offset
+    soft = jnp.maximum(score, LOG2E * jnp.log(1.0 + jnp.exp2(jnp.minimum(score, 126.0))))
     if visible is not None:
         soft = jnp.where(visible, soft, 0.0)
-    sums = jnp.dot(
-        jnp.concatenate(high_low(soft), axis=1), ladder, preferred_element_type=F32
-    )
-    behind = sums[:, :128] if fallen is None else sums[:, :128] + fallen
-    weight = jnp.exp2(score + behind)
+    soft = soft.astype(BF16)
+    last = jnp.dot(soft[:, 256:], ladder[:, :256], preferred_element_type=F32)
+    first = jnp.dot(soft[:, :256], ladder[:, :256], preferred_element_type=F32) + jnp.dot(
+        soft[:, 256:], ladder[:, 256:], preferred_element_type=F32
+    )
+    weight = jnp.exp2(score + jnp.concatenate([first, last], axis=1))
     if visible is not None:
         weight = jnp.where(visible, weight, 0.0)
-    portion = jnp.dot(weight.astype(BF16), value, preferred_element_type=F32)
-    total = sums[:, 128:] if fallen is None else sums[:, 128:] + fallen
-    return portion, total
+    return jnp.dot(weight.astype(BF16), values, preferred_element_type=F32), first[:, :128]
 
 
 def turned(gain, state):
@@ -162,21 +162,21 @@
             r_weight.at[kind, dx], {"fs": (x + dx) % NX},
         )
 
+    packed_copies = [
+        send(
+            remote(
+                packed.at[(y + dy) % NY], packed_in.at[y], s_packed.at[dy], r_packed.at[dy],
+                {"sp_1": (y + dy) % NY},
+            )
+        )
+        for dy in range(1, NY)
+    ]
     send(half_copy(0))
     for j in (1, 2, 3):
         send(row_copy(j))
     for kind in range(4):
         for dx in (1, 3, 2):
             send(weight_copy(kind, dx))
-    packed_copies = [
-        send(
-            remote(
-                packed.at[(y + dy) % NY], packed_in.at[y], s_packed.at[dy], r_packed.at[dy],
-                {"sp_1": (y + dy) % NY},
-            )
-        )
-        for dy in range(1, NY)
-    ]
     packed_in[y] = packed[y]
     rows_in[0, mine] = normed[...]
     keyed_w[depth, :128] = w_key[:, column]
@@ -246,9 +246,9 @@
                 new = powers_times((table_p[:n, cols], table_q[:n, cols]), by)
                 table_p[n : 2 * n, cols] = new[0]
                 table_q[n : 2 * n, cols] = new[1]
-    ladder_row = lax.broadcasted_iota(jnp.int32, (256, 256), 0) % 128
-    ladder_lane = lax.broadcasted_iota(jnp.int32, (256, 256), 1)
-    ladder[...] = jnp.where((ladder_lane >= 128) | (ladder_row >= ladder_lane), -1.0, 0.0).astype(
+    ladder_row = lax.broadcasted_iota(jnp.int32, (256, 512), 0)
+    ladder_lane = lax.broadcasted_iota(jnp.int32, (256, 512), 1)
+    ladder[...] = jnp.where((ladder_lane >= 256) | (ladder_row >= ladder_lane), -1.0, 0.0).astype(
         BF16
     )
 
@@ -272,19 +272,6 @@
             s_left.at[i - 1, j], r_left.at[i - 1, j], down,
         )
 
-    def own_keys(first, last):
-        product = jnp.dot(
-            rows_in[first:last].reshape((last - first) * 128, 2048), keyed_w[...],
-            preferred_element_type=F32,
-        ).astype(BF16)
-        for j in range(first, last):
-            own_in[block_of(j)] = product[(j - first) * 128 : (j - first + 1) * 128]
-            right_copy(1, j).start()
-            left_copy(1, j).start()
-
-    for j in (1, 2):
-        row_copy(j).wait_recv()
-        send(half_copy(j))
     for copy in packed_copies:
         copy.wait_recv()
     for b in range(NY):
@@ -300,16 +287,21 @@
         )
         for dz in range(1, NZ)
     ]
+    for j in (1, 2, 3):
+        row_copy(j).wait_recv()
+        send(half_copy(j))
     for kind in (0, 1):
         for dx in (1, 3, 2):
             weight_copy(kind, dx).wait_recv()
-    for j in (0, 1, 2):
+    for j in range(NY):
         half_copy(j).wait_recv()
-    own_keys(0, 3)
-    row_copy(3).wait_recv()
-    send(half_copy(3))
-    half_copy(3).wait_recv()
-    own_keys(3, 4)
+    product = jnp.dot(
+        rows_in[...].reshape(512, 2048), keyed_w[...], preferred_element_type=F32
+    ).astype(BF16)
+    for j in range(NY):
+        own_in[block_of(j)] = product[j * 128 : (j + 1) * 128]
+        right_copy(1, j).start()
+        left_copy(1, j).start()
     until = jnp.where(lane <= row, 1.0, 0.0)
     until_half = until.astype(BF16)
     falls = []
@@ -327,41 +319,46 @@
         weight_copy(2, dx).wait_recv()
     product = jnp.dot(
         rows_in[...].reshape(512, 2048), query_w[...], preferred_element_type=F32
-    ).astype(BF16)
+    )
+    product = (product * (LOG2E * 128**-0.5)).astype(BF16)
     for j in range(NY):
         queries[block_of(j)] = product[j * 128 : (j + 1) * 128]
 
-    def arrive(i, j):
-        right_copy(i, j).wait_recv()
-        left_copy(i, j).wait_recv()
-        if i < 3:
-            right_copy(i + 1, j).start()
-            left_copy(i + 1, j).start()
-            return
-
-        @pl.when(j < 2)
+    def arrive(i):
+        for j in range(NY):
+            if i < 4 or j < 2:
+                right_copy(i, j).wait_recv()
+                if i < 3 or i == 3 and j < 2:
+                    right_copy(i + 1, j).start()
+            if i < 4 or j >= 2:
+                left_copy(i, j).wait_recv()
+                if i < 3 or i == 3 and j >= 2:
+                    left_copy(i + 1, j).start()
+
+    def offset_row(dz):
+        return jnp.concatenate([offset_in[dz, b : b + 1, :] for b in range(NY)], axis=1)
+
+    def attend_far(dz, pairs):
+        @pl.when(z >= dz)
         def _():
-            right_copy(4, j).start()
-
-        @pl.when(j >= 2)
-        def _():
-            left_copy(4, j).start()
-
-    for j in range(NY):
-        arrive(1, j)
-
-    for q in range(NY):
-        portion_sum, fallen = None, None
-        for k in range(q, -1, -1):
-            portion, fallen = attend_pair(
-                queries[q], own_in[k, :, :128], own_in[k, :, 128:], offset_in[0, k : k + 1, :],
-                fallen, ladder[...], lane < row if k == q else None,
+            acc[dz], tot[dz] = attend_chunk(
+                queries[...].reshape(512, 128), pairs[...].reshape(512, 256), offset_row(dz),
+                ladder[...],
             )
-            portion_sum = portion if portion_sum is None else portion_sum + portion
-        acc[0, q] = portion_sum
-        tot[0, q] = fallen
+
+    def attend_step(i):
+        attend_far(i, right_in.at[i - 1])
+        attend_far(8 - i, left_in.at[i - 1])
+
+    acc[0], tot[0] = attend_chunk(
+        queries[...].reshape(512, 128), own_in[...].reshape(512, 256), offset_row(0), ladder[...],
+        lax.broadcasted_iota(jnp.int32, (512, 512), 1)
+        < lax.broadcasted_iota(jnp.int32, (512, 512), 0),
+    )
+    arrive(1)
     for copy in offset_copies:
         copy.wait_recv()
+    attend_step(1)
 
     for dx in (1, 3, 2):
         weight_copy(3, dx).wait_recv()
@@ -388,7 +385,6 @@
         falls[b] = jnp.exp(falls[b])
         ends[b] = falls[b] * turned(gain_last, ends[b])
         local = falls[b] * turned(gain_block, local) + ends[b]
-        arrive(2, b)
     state_own[:8, :] = local
     state_own[8:, :] = jnp.broadcast_to(fall_all, (8, 128))
     state_copies = [
@@ -401,47 +397,9 @@
         for dz in range(1, NZ)
     ]
 
-    def attend_block(dz, pairs, k):
-        offset = offset_in[dz, pl.ds(k, 1), :]
-        for q in range(NY):
-            portion, fallen = attend_pair(
-                queries[q], pairs[k, :, :128], pairs[k, :, 128:], offset, tot[dz, q],
-                ladder[...], None,
-            )
-            acc[dz, q] += portion
-            tot[dz, q] = fallen
-
-    def attend_step(i):
-        chunks = [(i, right_in.at[i - 1]), (8 - i, left_in.at[i - 1])] if i < 4 else [(4, far_in)]
-        for dz, _ in chunks:
-            @pl.when(z >= dz)
-            def _():
-                acc[dz] = jnp.zeros((NY, 128, 128), F32)
-                tot[dz] = jnp.zeros((NY, 128, 128), F32)
-
-        def one(turn, carry):
-            if i < 2:
-                arrive(i + 2, turn)
-            elif i == 2:
-                @pl.when(turn < 2)
-                def _():
-                    right_copy(4, turn).wait_recv()
-
-                @pl.when(turn >= 2)
-                def _():
-                    left_copy(4, turn).wait_recv()
-
-            for dz, pairs in chunks:
-                @pl.when(z >= dz)
-                def _():
-                    attend_block(dz, pairs, NY - 1 - turn)
-
-            return carry
-
-        lax.fori_loop(0, NY, one, 0)
-
-    attend_step(1)
+    arrive(2)
     attend_step(2)
+    arrive(3)
 
     for copy in state_copies:
         copy.wait_recv()
@@ -480,17 +438,16 @@
         send(copy)
     scan_in[0, 0] = scan_own[y]
     attend_step(3)
-    attend_step(4)
+    arrive(4)
+    attend_far(4, far_in)
     for dz in range(1, NZ):
         @pl.when(z >= dz)
         def _():
-            for q in range(NY):
-                fallen = tot[0, q]
-                acc[0, q] += jnp.exp2(fallen) * acc[dz, q]
-                tot[0, q] = fallen + tot[dz, q]
-
-    for q in range(NY):
-        attend_own[q] = acc[0, q].astype(BF16)
+            fallen = tot[0, :, :1]
+            acc[0] += jnp.exp2(fallen) * acc[dz]
+            tot[0, :, :1] = fallen + tot[dz, :, :1]
+
+    attend_own[...] = acc[0].astype(BF16).reshape(NY, 128, 128)
     attend_copies = spread_copies(attend_own, attend_in, s_attend, r_attend)
     for copy in attend_copies.values():
         send(copy)
@@ -568,9 +525,9 @@
             pltpu.VMEM((NZ, 8, 128), F32),
             pltpu.VMEM((16, 128), F32),
             pltpu.VMEM((NZ, 16, 128), F32),
-            pltpu.VMEM((NZ, NY, 128, 128), F32),
-            pltpu.VMEM((NZ, NY, 128, 128), F32),
-            pltpu.VMEM((256, 256), BF16),
+            pltpu.VMEM((NZ, 512, 128), F32),
+            pltpu.VMEM((NZ, 512, 128), F32),
+            pltpu.VMEM((256, 512), BF16),
             pltpu.VMEM((256, 2048), BF16),
             pltpu.VMEM((128, 2048), BF16),
             pltpu.VMEM((128, 1024), F32),

time: 86.1 us -> 77 us (0.89)
  the two profiles are of different devices: /device:TPU:225 before, /device:TPU:1 now
where the time goes in v4:
time: 77 us; the launch traced here: 76.9 us
  Pallas kernels  75 us (97%)
  other arithmetic  1.8 us (2%)
    pallas_call x1, Pallas kernels, layer(): pl.pallas_call(layer_kernel, out_shape=[jax.ShapeDtypeStruct((64, 2048),...  75 us
    broadcast_in_dim x1, other arithmetic, on_device(): return (parts[0].astype(F32) + parts[1].astype(F32)).astype(BF16)[None]  1.8 us

profile of v4, /device:TPU:1, one launch (start us, length us, event | category | flops | bytes accessed | tf_op | source)
XLA Modules:
  0.0 76.9 jit_solution(15216624527959008074)
XLA Ops:
  0.0 75.0 %layer.1 = (bf16[64,2048]{1,0:T(8,128)(2,1)}, bf16[64,2048]{1,0:T(8,128)(2,1)}) custom-call(bf16[64,2048]{1,0:T(8,128)(2,1)} %bitcast.11, f32[1,2048]{1,0:T(1,128)} %bitcast.14, bf16[512,512]{1,0:T(8,128)(2,1)} %refs_2_.1, bf16[512,512]{1,0:T(8,128)(2,1)} %refs_3_.1, bf16[512,512]{1,0:T(8,128)(2,1)} %refs_4_.1, bf16[512,512]{1,0:T(8,128)(2,1)} %refs_5_.1, ...), custom_call_target="tpu_custom_call" | custom-call | tf_op jit(solution)/shard_map/layer/pallas_call | solution.py:503
  75.1 1.8 %fusion = bf16[1,64,2048]{2,1,0:T(8,128)(2,1)} fusion(bf16[64,2048]{1,0:T(8,128)(2,1)} %get-tuple-element.8, bf16[64,2048]{1,0:T(8,128)(2,1)} %get-tuple-element.7), kind=kLoop, calls=%fused_computation.1 | loop fusion | flops 524288 | bytes 786432 | tf_op jit(solution)/shard_map/broadcast_in_dim | solution.py:580

commit v5 on v4

--- a/solution.py
+++ b/solution.py
@@ -83,31 +83,32 @@
 def layer_kernel(
     *refs,
 ):
-    operands, outs, held_here, rest = refs[:17], refs[17:19], refs[19:36], refs[36:]
-    run_layer(operands, outs, held_here, *rest)
+    operands, out, held_here, rest = refs[:17], refs[17], refs[18:35], refs[35:]
+    run_layer(operands, out, held_here, *rest)
 
 
 def run_layer(
-    operands, outs, held_here, s_operand,
+    operands, out, held_here, s_operand,
     normed, rows_in, keyed_w, query_w, drive_w, packed, packed_in, driven_in, queries,
     own_in, right_in, left_in, far_in, offset_own, offset_in, state_own, state_in, acc, tot,
     ladder, into_map, out_map, fwd_p, fwd_q, inv_p, inv_q, held, ends, decay,
-    attend_own, scan_own, attend_in, scan_in, part_out, part_in,
+    attend_own, scan_own, attend_in, scan_in, part_out, part_in, product_own, half_out, half_in,
     s_rows, r_rows, s_half, r_half, s_weight, r_weight, s_packed, r_packed,
     s_right, r_right, s_left, r_left, s_offset, r_offset, s_state, r_state,
-    s_attend, r_attend, s_scan, r_scan, s_part, r_part,
+    s_scan, r_scan, s_part, r_part, s_slice, r_slice, s_relay, r_relay, s_attend, r_attend,
+    s_last, r_last,
 ):
     (
         tok, gain_ref, w_drive, w_query, w_key, w_value, key_offset, log_step_ref, lambda_real,
         lambda_imag, input_map, output_map, skip_ref, forget_ref, initial_ref, w_attend, w_scan,
     ) = held_here
+    z, y, x, t = (lax.axis_index(a) for a in ("sp_0", "sp_1", "fs", "tp"))
     fetches = [
-        pltpu.make_async_copy(src, dst, s_operand.at[k])
+        pltpu.make_async_copy(src, dst.at[x] if k == 15 else dst, s_operand.at[k])
         for k, (src, dst) in enumerate(zip(operands, held_here))
     ]
     for fetch in fetches:
         fetch.start()
-    z, y, x, t = (lax.axis_index(a) for a in ("sp_0", "sp_1", "fs", "tp"))
     greet(plane_peers(x, y, t) + [{"sp_0": (z + dz) % NZ} for dz in range(1, NZ)])
     row = lax.broadcasted_iota(jnp.int32, (128, 128), 0)
     lane = lax.broadcasted_iota(jnp.int32, (128, 128), 1)
@@ -129,7 +130,7 @@
     values = tok[...].astype(F32)
     scale = lax.rsqrt(jnp.mean(values * values, axis=1, keepdims=True) + EPSILON)
     normed[...] = (values * scale * gain_ref[...]).astype(BF16)
-    for k in (2, 3, 4, 5):
+    for k in (2, 3, 4, 5, 15):
         fetches[k].wait()
     await_greetings(26)
 
@@ -160,6 +161,18 @@
         return remote(
             sources[kind].at[:, column], targets[kind], s_weight.at[kind, dx],
             r_weight.at[kind, dx], {"fs": (x + dx) % NX},
+        )
+
+    def slice_copy(dx):
+        return remote(
+            w_attend.at[x, column], w_attend.at[x, column], s_slice.at[dx], r_slice.at[dx],
+            {"fs": (x + dx) % NX},
+        )
+
+    def relay_copy(dx, dy):
+        part = w_attend.at[(x + NX - dx) % NX, column]
+        return remote(
+            part, part, s_relay.at[dx, dy], r_relay.at[dx, dy], {"sp_1": (y + dy) % NY}
         )
 
     packed_copies = [
@@ -174,9 +187,9 @@
     send(half_copy(0))
     for j in (1, 2, 3):
         send(row_copy(j))
-    for kind in range(4):
+    for kind in (0, 1, None, 3, 2):
         for dx in (1, 3, 2):
-            send(weight_copy(kind, dx))
+            send(slice_copy(dx) if kind is None else weight_copy(kind, dx))
     packed_in[y] = packed[y]
     rows_in[0, mine] = normed[...]
     keyed_w[depth, :128] = w_key[:, column]
@@ -184,7 +197,7 @@
     query_w[depth] = w_query[:, column]
     drive_w[depth] = w_drive[:, column]
 
-    for k in (7, 8, 9, 10, 11, 12, 14, 15, 16):
+    for k in (7, 8, 9, 10, 11, 12, 14, 16):
         fetches[k].wait()
     sign = jnp.where(lane[:8] < 64, -1.0, 1.0)
     groups = pl.ds(pl.multiple_of(y * 8, 8), 8)
@@ -316,16 +329,12 @@
         )
         falls.append(jnp.sum(forget, axis=1, keepdims=True))
     for dx in (1, 3, 2):
-        weight_copy(2, dx).wait_recv()
-    product = jnp.dot(
-        rows_in[...].reshape(512, 2048), query_w[...], preferred_element_type=F32
-    )
-    product = (product * (LOG2E * 128**-0.5)).astype(BF16)
-    for j in range(NY):
-        queries[block_of(j)] = product[j * 128 : (j + 1) * 128]
-
-    def arrive(i):
-        for j in range(NY):
+        slice_copy(dx).wait_recv()
+        for dy in (1, 3, 2):
+            send(relay_copy(dx, dy))
+
+    def arrive(i, blocks=range(NY)):
+        for j in blocks:
             if i < 4 or j < 2:
                 right_copy(i, j).wait_recv()
                 if i < 3 or i == 3 and j < 2:
@@ -350,15 +359,7 @@
         attend_far(i, right_in.at[i - 1])
         attend_far(8 - i, left_in.at[i - 1])
 
-    acc[0], tot[0] = attend_chunk(
-        queries[...].reshape(512, 128), own_in[...].reshape(512, 256), offset_row(0), ladder[...],
-        lax.broadcasted_iota(jnp.int32, (512, 512), 1)
-        < lax.broadcasted_iota(jnp.int32, (512, 512), 0),
-    )
     arrive(1)
-    for copy in offset_copies:
-        copy.wait_recv()
-    attend_step(1)
 
     for dx in (1, 3, 2):
         weight_copy(3, dx).wait_recv()
@@ -385,6 +386,7 @@
         falls[b] = jnp.exp(falls[b])
         ends[b] = falls[b] * turned(gain_last, ends[b])
         local = falls[b] * turned(gain_block, local) + ends[b]
+        arrive(2, (b,))
     state_own[:8, :] = local
     state_own[8:, :] = jnp.broadcast_to(fall_all, (8, 128))
     state_copies = [
@@ -397,9 +399,23 @@
         for dz in range(1, NZ)
     ]
 
-    arrive(2)
-    attend_step(2)
-    arrive(3)
+    for dx in (1, 3, 2):
+        weight_copy(2, dx).wait_recv()
+    product = jnp.dot(
+        rows_in[...].reshape(512, 2048), query_w[...], preferred_element_type=F32
+    )
+    product = (product * (LOG2E * 128**-0.5)).astype(BF16)
+    for j in range(NY):
+        queries[block_of(j)] = product[j * 128 : (j + 1) * 128]
+
+    acc[0], tot[0] = attend_chunk(
+        queries[...].reshape(512, 128), own_in[...].reshape(512, 256), offset_row(0), ladder[...],
+        lax.broadcasted_iota(jnp.int32, (512, 512), 1)
+        < lax.broadcasted_iota(jnp.int32, (512, 512), 0),
+    )
+    for copy in offset_copies:
+        copy.wait_recv()
+    arrive(3, (0, 1))
 
     for copy in state_copies:
         copy.wait_recv()
@@ -437,21 +453,36 @@
     for copy in scan_copies.values():
         send(copy)
     scan_in[0, 0] = scan_own[y]
-    attend_step(3)
+    arrive(3, (2, 3))
+    for i in (1, 2, 3):
+        attend_step(i)
+
+    def join(near, far):
+        @pl.when(z >= far)
+        def _():
+            fallen = tot[near, :, :1]
+            acc[near] += jnp.exp2(fallen) * acc[far]
+            tot[near, :, :1] = fallen + tot[far, :, :1]
+
+    for dz in (1, 2, 3):
+        join(0, dz)
+    for dz in (6, 7):
+        join(5, dz)
     arrive(4)
     attend_far(4, far_in)
-    for dz in range(1, NZ):
-        @pl.when(z >= dz)
-        def _():
-            fallen = tot[0, :, :1]
-            acc[0] += jnp.exp2(fallen) * acc[dz]
-            tot[0, :, :1] = fallen + tot[dz, :, :1]
-
+    for dz in (4, 5):
+        join(0, dz)
     attend_own[...] = acc[0].astype(BF16).reshape(NY, 128, 128)
-    attend_copies = spread_copies(attend_own, attend_in, s_attend, r_attend)
-    for copy in attend_copies.values():
-        send(copy)
-    attend_in[0, 0] = attend_own[y]
+    attend_copies = [
+        send(
+            remote(
+                attend_own.at[(y + dy) % NY], attend_in.at[:, column], s_attend.at[dy],
+                r_attend.at[dy], {"sp_1": (y + dy) % NY},
+            )
+        )
+        for dy in (1, 3, 2)
+    ]
+    attend_in[:, column] = attend_own[y]
 
     part_copies = {}
     for dx in order:
@@ -459,12 +490,9 @@
         for dy in range(NY):
             if (dx, dy) != (0, 0):
                 scan_copies[dx, dy].wait_recv()
-                attend_copies[dx, dy].wait_recv()
             head = (y + NY - dy) % NY
             head_rows = pl.ds(pl.multiple_of(head * 128, 128), 128)
-            product = jnp.dot(
-                attend_in[dx, dy], w_attend[head_rows, :], preferred_element_type=F32
-            ) + jnp.dot(scan_in[dx, dy], w_scan[head_rows, :], preferred_element_type=F32)
+            product = jnp.dot(scan_in[dx, dy], w_scan[head_rows, :], preferred_element_type=F32)
             total = product if total is None else total + product
         rounded = total.astype(BF16)
         for k in range(NT):
@@ -479,13 +507,29 @@
                     )
                 )
     part_in[0, 0] = part_out[0, t]
+    for dx in (1, 3, 2):
+        for dy in (1, 3, 2):
+            relay_copy(dx, dy).wait_recv()
+    for copy in attend_copies:
+        copy.wait_recv()
+    other = pl.ds(pl.multiple_of((1 - t) * 64, 64), 64)
+    last_copies = []
+    for k in range(NX):
+        product_own[k] = jnp.dot(attend_in[...], w_attend[k], preferred_element_type=F32)
+        half_out[k] = product_own[k, other, :].astype(BF16)
+        last_copies.append(
+            send(remote(half_out.at[k], half_in.at[k], s_last.at[k], r_last.at[k], sibling))
+        )
+    for copy in last_copies:
+        copy.wait_recv()
     for dx in order:
         for dt in range(NT):
             if (dx, dt) != (0, 0):
                 part_copies[dx, dt].wait_recv()
-        columns = pl.ds(pl.multiple_of((x + dx) % NX * 512, 512), 512)
-        for dt in range(NT):
-            outs[dt][:, columns] = part_in[dx, dt]
+        k = (x + dx) % NX
+        columns = pl.ds(pl.multiple_of(k * 512, 512), 512)
+        scan_part = part_in[dx, 0].astype(F32) + part_in[dx, 1].astype(F32)
+        out[:, columns] = (product_own[k, mine, :] + half_in[k].astype(F32) + scan_part).astype(BF16)
     for copy in sent:
         copy.wait_send()
     for i in range(1, 5):
@@ -502,11 +546,14 @@
 
     return pl.pallas_call(
         layer_kernel,
-        out_shape=[jax.ShapeDtypeStruct((64, 2048), BF16)] * NT,
+        out_shape=pltpu.VMEM((64, 2048), BF16),
         in_specs=[pl.BlockSpec(memory_space=pl.ANY)] * 17,
-        out_specs=[VMEM] * NT,
+        out_specs=VMEM,
         scratch_shapes=[
-            *(pltpu.VMEM(operand.shape, operand.dtype) for operand in operands),
+            *(
+                pltpu.VMEM((NX, 512, 512) if k == 15 else operand.shape, operand.dtype)
+                for k, operand in enumerate(operands)
+            ),
             pltpu.SemaphoreType.DMA((17,)),
             pltpu.VMEM((64, 2048), BF16),
             pltpu.VMEM((NY, 128, 2048), BF16),
@@ -539,12 +586,15 @@
             pltpu.VMEM((NY, 128, 128), F32),
             pltpu.VMEM((NY, 128, 128), BF16),
             pltpu.VMEM((NY, 128, 128), BF16),
-            pltpu.VMEM((NX, NY, 128, 128), BF16),
+            pltpu.VMEM((128, 512), BF16),
             pltpu.VMEM((NX, NY, 128, 128), BF16),
             pltpu.VMEM((NX, NT, 64, 512), BF16),
             pltpu.VMEM((NX, NT, 64, 512), BF16),
+            pltpu.VMEM((NX, 128, 512), F32),
+            pltpu.VMEM((NX, 64, 512), BF16),
+            pltpu.VMEM((NX, 64, 512), BF16),
             *sems(NY), *sems(NY), *sems(4, NX), *sems(NY), *sems(4, NY), *sems(4, NY), *sems(NZ),
-            *sems(NZ), *sems(NX, NY), *sems(NX, NY), *sems(NX, NT),
+            *sems(NZ), *sems(NX, NY), *sems(NX, NT), *sems(NX), *sems(NX, NY), *sems(NY), *sems(NX),
         ],
         compiler_params=pltpu.CompilerParams(
             collective_id=0, has_side_effects=True, vmem_limit_bytes=60 << 20
@@ -558,7 +608,7 @@
     lambda_real, lambda_imag, input_map, output_map, skip_gain, forget, initial_state,
     scan_out_weight, attend_out_weight,
 ):
-    parts = layer(
+    return layer(
         tokens[0],
         norm_gain[None],
         drive_weight,
@@ -576,8 +626,7 @@
         initial_state[:, 0],
         attend_out_weight,
         scan_out_weight,
-    )
-    return (parts[0].astype(F32) + parts[1].astype(F32)).astype(BF16)[None]
+    )[None]
 
 
 def solution(mesh):

time: 77 us -> 68.1 us (0.88)
  Pallas kernels: 75 us -> 67.3 us
  other arithmetic: 1.8 us -> 0 us
    pallas_call x1, Pallas kernels: 75 us -> 67.3 us  [layer(): pl.pallas_call(layer_kernel, out_shape=pltpu.VMEM((64, 2048), BF16), in_s...]
    broadcast_in_dim x1 -> x0, other arithmetic: 1.8 us -> none  [on_device(): return (parts[0].astype(F32) + parts[1].astype(F32)).astype(BF16)[None]]
where the time goes in v5:
time: 68.1 us; the launch traced here: 68 us
  Pallas kernels  67.3 us (99%)
  local copies, waits for them, and re-layouts  0.71 us (1%)
    pallas_call x1, Pallas kernels, layer(): pl.pallas_call(layer_kernel, out_shape=pltpu.VMEM((64, 2048), BF16), in_s...  67.3 us

profile of v5, /device:TPU:1, one launch (start us, length us, event | category | flops | bytes accessed | tf_op | source)
XLA Modules:
  0.0 68.0 jit_solution(1155626047075166897)
XLA Ops:
  0.0 67.3 %layer.1 = bf16[64,2048]{1,0:T(8,128)(2,1)S(1)} custom-call(bf16[64,2048]{1,0:T(8,128)(2,1)} %bitcast.11, f32[1,2048]{1,0:T(1,128)} %bitcast.14, bf16[512,512]{1,0:T(8,128)(2,1)} %refs_2_.1, bf16[512,512]{1,0:T(8,128)(2,1)} %refs_3_.1, bf16[512,512]{1,0:T(8,128)(2,1)} %refs_4_.1, bf16[512,512]{1,0:T(8,128)(2,1)} %refs_5_.1, bf16[4,128]{1,0:T(4,128)(2,1)} %bitcast.16, ...), custom_call_target="tpu_custom_call" | custom-call | tf_op jit(solution)/shard_map/layer/pallas_call | solution.py:547
  67.3 0.7 %copy.19 = bf16[1,64,2048]{2,1,0:T(8,128)(2,1)} copy(bf16[1,64,2048]{2,1,0:T(8,128)(2,1)S(1)} %bitcast.9) | data formatting | bytes 524288

commit v6 on v5

--- a/solution.py
+++ b/solution.py
@@ -96,7 +96,7 @@
     s_rows, r_rows, s_half, r_half, s_weight, r_weight, s_packed, r_packed,
     s_right, r_right, s_left, r_left, s_offset, r_offset, s_state, r_state,
     s_scan, r_scan, s_part, r_part, s_slice, r_slice, s_relay, r_relay, s_attend, r_attend,
-    s_last, r_last,
+    s_last, r_last, s_drive, r_drive, s_share, r_share,
 ):
     (
         tok, gain_ref, w_drive, w_query, w_key, w_value, key_offset, log_step_ref, lambda_real,
@@ -152,15 +152,28 @@
 
     column = pl.ds(pl.multiple_of(y * 128, 128), 128)
     depth = pl.ds(pl.multiple_of(x * 512, 512), 512)
-    sources = (w_key, w_value, w_query, w_drive)
-    targets = (
-        keyed_w.at[depth, :128], keyed_w.at[depth, 128:], query_w.at[depth], drive_w.at[depth]
-    )
+    sources = (w_key, w_value, w_query)
+    targets = (keyed_w.at[depth, :128], keyed_w.at[depth, 128:], query_w.at[depth])
 
     def weight_copy(kind, dx):
         return remote(
             sources[kind].at[:, column], targets[kind], s_weight.at[kind, dx],
             r_weight.at[kind, dx], {"fs": (x + dx) % NX},
+        )
+
+    def eighth(k):
+        return drive_w.at[pl.ds(pl.multiple_of(k * 512 + z * 64, 64), 64)]
+
+    def drive_copy(dx):
+        return remote(
+            w_drive.at[pl.ds(pl.multiple_of(z * 64, 64), 64), column], eighth(x), s_drive.at[dx],
+            r_drive.at[dx], {"fs": (x + dx) % NX},
+        )
+
+    def share_copy(dx, dz):
+        part = eighth((x + NX - dx) % NX)
+        return remote(
+            part, part, s_share.at[dx, dz], r_share.at[dx, dz], {"sp_0": (z + dz) % NZ}
         )
 
     def slice_copy(dx):
@@ -187,7 +200,9 @@
     send(half_copy(0))
     for j in (1, 2, 3):
         send(row_copy(j))
-    for kind in (0, 1, None, 3, 2):
+    for dx in (1, 3, 2):
+        send(drive_copy(dx))
+    for kind in (0, 1, None, 2):
         for dx in (1, 3, 2):
             send(slice_copy(dx) if kind is None else weight_copy(kind, dx))
     packed_in[y] = packed[y]
@@ -300,6 +315,23 @@
         )
         for dz in range(1, NZ)
     ]
+    for dx in (1, 3, 2):
+        drive_copy(dx).wait_recv()
+        for dz in (1, 7, 2, 6, 3, 5, 4):
+            send(share_copy(dx, dz))
+    until = jnp.where(lane <= row, 1.0, 0.0)
+    until_half = until.astype(BF16)
+    falls = []
+    for b in range(NY):
+        forget = packed_in[b, :8, :]
+        spread = jnp.concatenate(
+            [jnp.broadcast_to(forget[g : g + 1], (16, 128)) for g in range(8)], axis=0
+        )
+        decay[b] = lax.dot_general(
+            until, spread, (((1,), (1,)), ((), ())), preferred_element_type=F32,
+            precision=lax.Precision.HIGHEST,
+        )
+        falls.append(jnp.sum(forget, axis=1, keepdims=True))
     for j in (1, 2, 3):
         row_copy(j).wait_recv()
         send(half_copy(j))
@@ -315,24 +347,6 @@
         own_in[block_of(j)] = product[j * 128 : (j + 1) * 128]
         right_copy(1, j).start()
         left_copy(1, j).start()
-    until = jnp.where(lane <= row, 1.0, 0.0)
-    until_half = until.astype(BF16)
-    falls = []
-    for b in range(NY):
-        forget = packed_in[b, :8, :]
-        spread = jnp.concatenate(
-            [jnp.broadcast_to(forget[g : g + 1], (16, 128)) for g in range(8)], axis=0
-        )
-        decay[b] = lax.dot_general(
-            until, spread, (((1,), (1,)), ((), ())), preferred_element_type=F32,
-            precision=lax.Precision.HIGHEST,
-        )
-        falls.append(jnp.sum(forget, axis=1, keepdims=True))
-    for dx in (1, 3, 2):
-        slice_copy(dx).wait_recv()
-        for dy in (1, 3, 2):
-            send(relay_copy(dx, dy))
-
     def arrive(i, blocks=range(NY)):
         for j in blocks:
             if i < 4 or j < 2:
@@ -359,10 +373,14 @@
         attend_far(i, right_in.at[i - 1])
         attend_far(8 - i, left_in.at[i - 1])
 
-    arrive(1)
+    def pass_slice(dx):
+        slice_copy(dx).wait_recv()
+        for dy in (1, 3, 2):
+            send(relay_copy(dx, dy))
 
     for dx in (1, 3, 2):
-        weight_copy(3, dx).wait_recv()
+        for dz in range(1, NZ):
+            share_copy(dx, dz).wait_recv()
     product = jnp.dot(
         rows_in[...].reshape(512, 2048), drive_w[...], preferred_element_type=F32
     ).astype(BF16)
@@ -386,7 +404,10 @@
         falls[b] = jnp.exp(falls[b])
         ends[b] = falls[b] * turned(gain_last, ends[b])
         local = falls[b] * turned(gain_block, local) + ends[b]
-        arrive(2, (b,))
+        if b == 1:
+            pass_slice(1)
+        elif b > 1:
+            arrive(1, (b - 2,))
     state_own[:8, :] = local
     state_own[8:, :] = jnp.broadcast_to(fall_all, (8, 128))
     state_copies = [
@@ -399,6 +420,8 @@
         for dz in range(1, NZ)
     ]
 
+    arrive(1, (2, 3))
+    pass_slice(3)
     for dx in (1, 3, 2):
         weight_copy(2, dx).wait_recv()
     product = jnp.dot(
@@ -408,6 +431,7 @@
     for j in range(NY):
         queries[block_of(j)] = product[j * 128 : (j + 1) * 128]
 
+    arrive(2, (0, 1))
     acc[0], tot[0] = attend_chunk(
         queries[...].reshape(512, 128), own_in[...].reshape(512, 256), offset_row(0), ladder[...],
         lax.broadcasted_iota(jnp.int32, (512, 512), 1)
@@ -415,7 +439,9 @@
     )
     for copy in offset_copies:
         copy.wait_recv()
-    arrive(3, (0, 1))
+    arrive(2, (2,))
+    attend_step(1)
+    arrive(2, (3,))
 
     for copy in state_copies:
         copy.wait_recv()
@@ -453,9 +479,11 @@
     for copy in scan_copies.values():
         send(copy)
     scan_in[0, 0] = scan_own[y]
+    pass_slice(2)
+    arrive(3, (0, 1))
+    attend_step(2)
     arrive(3, (2, 3))
-    for i in (1, 2, 3):
-        attend_step(i)
+    attend_step(3)
 
     def join(near, far):
         @pl.when(z >= far)
@@ -593,8 +621,9 @@
             pltpu.VMEM((NX, 128, 512), F32),
             pltpu.VMEM((NX, 64, 512), BF16),
             pltpu.VMEM((NX, 64, 512), BF16),
-            *sems(NY), *sems(NY), *sems(4, NX), *sems(NY), *sems(4, NY), *sems(4, NY), *sems(NZ),
+            *sems(NY), *sems(NY), *sems(3, NX), *sems(NY), *sems(4, NY), *sems(4, NY), *sems(NZ),
             *sems(NZ), *sems(NX, NY), *sems(NX, NT), *sems(NX), *sems(NX, NY), *sems(NY), *sems(NX),
+            *sems(NX), *sems(NX, NZ),
         ],
         compiler_params=pltpu.CompilerParams(
             collective_id=0, has_side_effects=True, vmem_limit_bytes=60 << 20

time: 68.1 us -> 65.7 us (0.965)
  Pallas kernels: 67.3 us -> 65 us
    pallas_call x1, Pallas kernels: 67.3 us -> 65 us  [layer(): pl.pallas_call(layer_kernel, out_shape=pltpu.VMEM((64, 2048), BF16), in_s...]
where the time goes in v6:
time: 65.7 us
  Pallas kernels  65 us (99%)
  local copies, waits for them, and re-layouts  0.71 us (1%)
    pallas_call x1, Pallas kernels, layer(): pl.pallas_call(layer_kernel, out_shape=pltpu.VMEM((64, 2048), BF16), in_s...  65 us

profile of v6, /device:TPU:1, one launch (start us, length us, event | category | flops | bytes accessed | tf_op | source)
XLA Modules:
  0.0 65.7 jit_solution(10501042569736069958)
XLA Ops:
  0.0 65.0 %layer.1 = bf16[64,2048]{1,0:T(8,128)(2,1)S(1)} custom-call(bf16[64,2048]{1,0:T(8,128)(2,1)} %bitcast.11, f32[1,2048]{1,0:T(1,128)} %bitcast.14, bf16[512,512]{1,0:T(8,128)(2,1)} %refs_2_.1, bf16[512,512]{1,0:T(8,128)(2,1)} %refs_3_.1, bf16[512,512]{1,0:T(8,128)(2,1)} %refs_4_.1, bf16[512,512]{1,0:T(8,128)(2,1)} %refs_5_.1, bf16[4,128]{1,0:T(4,128)(2,1)} %bitcast.16, ...), custom_call_target="tpu_custom_call" | custom-call | tf_op jit(solution)/shard_map/layer/pallas_call | solution.py:575
  65.0 0.7 %copy.19 = bf16[1,64,2048]{2,1,0:T(8,128)(2,1)} copy(bf16[1,64,2048]{2,1,0:T(8,128)(2,1)S(1)} %bitcast.9) | data formatting | bytes 524288

commit v7 on v6

--- a/solution.py
+++ b/solution.py
@@ -14,6 +14,11 @@
 LOG2E = 1.4426950408889634
 NZ, NY, NX, NT = 8, 4, 4, 2
 BF16, F32 = jnp.bfloat16, jnp.float32
+TOGETHER = (
+    "half", "keyed", "query", "packed", "offset", "state", "scan", "pre", "part", "hop", "attend",
+    "last", "share",
+)
+SENT = TOGETHER + ("rows", "right", "left", "slice", "relay", "drive")
 VMEM = pl.BlockSpec(memory_space=pltpu.VMEM)
 MESH_ID = pl.DeviceIdType.MESH
 
@@ -93,10 +98,8 @@
     own_in, right_in, left_in, far_in, offset_own, offset_in, state_own, state_in, acc, tot,
     ladder, into_map, out_map, fwd_p, fwd_q, inv_p, inv_q, held, ends, decay,
     attend_own, scan_own, attend_in, scan_in, part_out, part_in, product_own, half_out, half_in,
-    s_rows, r_rows, s_half, r_half, s_weight, r_weight, s_packed, r_packed,
-    s_right, r_right, s_left, r_left, s_offset, r_offset, s_state, r_state,
-    s_scan, r_scan, s_part, r_part, s_slice, r_slice, s_relay, r_relay, s_attend, r_attend,
-    s_last, r_last, s_drive, r_drive, s_share, r_share,
+    scan_product, pre_out, pre_in,
+    s_all, r_all, r_rows, r_right, r_left, r_slice, r_relay, r_drive,
 ):
     (
         tok, gain_ref, w_drive, w_query, w_key, w_value, key_offset, log_step_ref, lambda_real,
@@ -113,12 +116,15 @@
     row = lax.broadcasted_iota(jnp.int32, (128, 128), 0)
     lane = lax.broadcasted_iota(jnp.int32, (128, 128), 1)
     up, down = {"sp_0": (z + 1) % NZ}, {"sp_0": (z + NZ - 1) % NZ}
-    sent = []
+    s_of = {name: s_all.at[k] for k, name in enumerate(SENT)}
+    r_of = {name: r_all.at[k] for k, name in enumerate(TOGETHER)}
 
     def send(copy):
         copy.start()
-        sent.append(copy)
         return copy
+
+    def await_all(name, data):
+        remote(data, data, s_of[name], r_of[name], sibling).wait_recv()
 
     for k in (0, 1, 6, 13):
         fetches[k].wait()
@@ -140,13 +146,13 @@
 
     def row_copy(j):
         return remote(
-            normed, rows_in.at[j, mine], s_rows.at[j], r_rows.at[j],
+            normed, rows_in.at[j, mine], s_of["rows"], r_rows.at[j - 1],
             {"sp_1": (y + order[j]) % NY},
         )
 
     def half_copy(j):
         return remote(
-            rows_in.at[j, mine] if j else normed, rows_in.at[j, mine], s_half.at[j], r_half.at[j],
+            rows_in.at[j, mine] if j else normed, rows_in.at[j, mine], s_of["half"], r_of["half"],
             sibling,
         )
 
@@ -156,9 +162,10 @@
     targets = (keyed_w.at[depth, :128], keyed_w.at[depth, 128:], query_w.at[depth])
 
     def weight_copy(kind, dx):
-        return remote(
-            sources[kind].at[:, column], targets[kind], s_weight.at[kind, dx],
-            r_weight.at[kind, dx], {"fs": (x + dx) % NX},
+        group = "query" if kind == 2 else "keyed"
+        return remote(
+            sources[kind].at[:, column], targets[kind], s_of[group], r_of[group],
+            {"fs": (x + dx) % NX},
         )
 
     def eighth(k):
@@ -166,37 +173,42 @@
 
     def drive_copy(dx):
         return remote(
-            w_drive.at[pl.ds(pl.multiple_of(z * 64, 64), 64), column], eighth(x), s_drive.at[dx],
-            r_drive.at[dx], {"fs": (x + dx) % NX},
+            w_drive.at[pl.ds(pl.multiple_of(z * 64, 64), 64), column], eighth(x), s_of["drive"],
+            r_drive.at[dx - 1], {"fs": (x + dx) % NX},
         )
 
     def share_copy(dx, dz):
         part = eighth((x + NX - dx) % NX)
         return remote(
-            part, part, s_share.at[dx, dz], r_share.at[dx, dz], {"sp_0": (z + dz) % NZ}
+            part, part, s_of["share"], r_of["share"], {"sp_0": (z + dz) % NZ}
         )
 
     def slice_copy(dx):
         return remote(
-            w_attend.at[x, column], w_attend.at[x, column], s_slice.at[dx], r_slice.at[dx],
+            w_attend.at[x, column], w_attend.at[x, column], s_of["slice"], r_slice.at[dx - 1],
             {"fs": (x + dx) % NX},
         )
 
     def relay_copy(dx, dy):
         part = w_attend.at[(x + NX - dx) % NX, column]
         return remote(
-            part, part, s_relay.at[dx, dy], r_relay.at[dx, dy], {"sp_1": (y + dy) % NY}
-        )
-
-    packed_copies = [
+            part, part, s_of["relay"], r_relay.at[dx - 1, dy // 2], {"sp_1": (y + dy) % NY}
+        )
+
+    def hop_copy(dx, dy):
+        start = (y + NY - dy) % NY * 128 + dy // 2 * 64
+        part = w_attend.at[
+            (x + NX - dx) % NX, pl.ds(pl.multiple_of(start, 64), 64)
+        ]
+        return remote(part, part, s_of["hop"], r_of["hop"], {"sp_1": (y + dy) % NY})
+
+    for dy in range(1, NY):
         send(
             remote(
-                packed.at[(y + dy) % NY], packed_in.at[y], s_packed.at[dy], r_packed.at[dy],
+                packed.at[(y + dy) % NY], packed_in.at[y], s_of["packed"], r_of["packed"],
                 {"sp_1": (y + dy) % NY},
             )
         )
-        for dy in range(1, NY)
-    ]
     send(half_copy(0))
     for j in (1, 2, 3):
         send(row_copy(j))
@@ -289,7 +301,7 @@
         return remote(
             own_in.at[b] if i == 1 else right_in.at[i - 2, b],
             far_in.at[b] if i == 4 else right_in.at[i - 1, b],
-            s_right.at[i - 1, j], r_right.at[i - 1, j], up,
+            s_of["right"], r_right.at[4 * i - 4 + j], up,
         )
 
     def left_copy(i, j):
@@ -297,24 +309,21 @@
         return remote(
             own_in.at[b] if i == 1 else left_in.at[i - 2, b],
             far_in.at[b] if i == 4 else left_in.at[i - 1, b],
-            s_left.at[i - 1, j], r_left.at[i - 1, j], down,
-        )
-
-    for copy in packed_copies:
-        copy.wait_recv()
+            s_of["left"], r_left.at[4 * i - 4 + j - (2 if i == 4 else 0)], down,
+        )
+
+    await_all("packed", packed_in.at[:3])
     for b in range(NY):
         offset_own[b : b + 1, :] = packed_in[b, 8:9, :]
         offset_in[0, b : b + 1, :] = packed_in[b, 8:9, :]
     offset_own[4:8, :] = jnp.zeros((4, 128), F32)
-    offset_copies = [
+    for dz in range(1, NZ):
         send(
             remote(
-                offset_own, offset_in.at[dz], s_offset.at[dz], r_offset.at[dz],
+                offset_own, offset_in.at[dz], s_of["offset"], r_of["offset"],
                 {"sp_0": (z + dz) % NZ},
             )
         )
-        for dz in range(1, NZ)
-    ]
     for dx in (1, 3, 2):
         drive_copy(dx).wait_recv()
         for dz in (1, 7, 2, 6, 3, 5, 4):
@@ -335,11 +344,8 @@
     for j in (1, 2, 3):
         row_copy(j).wait_recv()
         send(half_copy(j))
-    for kind in (0, 1):
-        for dx in (1, 3, 2):
-            weight_copy(kind, dx).wait_recv()
-    for j in range(NY):
-        half_copy(j).wait_recv()
+    await_all("keyed", keyed_w.at[:1536])
+    await_all("half", rows_in.at[:2])
     product = jnp.dot(
         rows_in[...].reshape(512, 2048), keyed_w[...], preferred_element_type=F32
     ).astype(BF16)
@@ -375,12 +381,15 @@
 
     def pass_slice(dx):
         slice_copy(dx).wait_recv()
-        for dy in (1, 3, 2):
+        for dy in (1, 3):
             send(relay_copy(dx, dy))
 
-    for dx in (1, 3, 2):
-        for dz in range(1, NZ):
-            share_copy(dx, dz).wait_recv()
+    def pass_on(dx):
+        for dy in (1, 3):
+            relay_copy(dx, dy).wait_recv()
+            send(hop_copy(dx, dy))
+
+    await_all("share", drive_w.at[:1344])
     product = jnp.dot(
         rows_in[...].reshape(512, 2048), drive_w[...], preferred_element_type=F32
     ).astype(BF16)
@@ -408,22 +417,21 @@
             pass_slice(1)
         elif b > 1:
             arrive(1, (b - 2,))
+    pass_slice(3)
     state_own[:8, :] = local
     state_own[8:, :] = jnp.broadcast_to(fall_all, (8, 128))
-    state_copies = [
+    for dz in range(1, NZ):
         send(
             remote(
-                state_own, state_in.at[dz], s_state.at[dz], r_state.at[dz],
+                state_own, state_in.at[dz], s_of["state"], r_of["state"],
                 {"sp_0": (z + dz) % NZ},
             )
         )
-        for dz in range(1, NZ)
-    ]
 
     arrive(1, (2, 3))
-    pass_slice(3)
-    for dx in (1, 3, 2):
-        weight_copy(2, dx).wait_recv()
+    pass_slice(2)
+    pass_on(1)
+    await_all("query", query_w.at[:1536])
     product = jnp.dot(
         rows_in[...].reshape(512, 2048), query_w[...], preferred_element_type=F32
     )
@@ -432,19 +440,16 @@
         queries[block_of(j)] = product[j * 128 : (j + 1) * 128]
 
     arrive(2, (0, 1))
+    pass_on(3)
     acc[0], tot[0] = attend_chunk(
         queries[...].reshape(512, 128), own_in[...].reshape(512, 256), offset_row(0), ladder[...],
         lax.broadcasted_iota(jnp.int32, (512, 512), 1)
         < lax.broadcasted_iota(jnp.int32, (512, 512), 0),
     )
-    for copy in offset_copies:
-        copy.wait_recv()
-    arrive(2, (2,))
-    attend_step(1)
-    arrive(2, (3,))
-
-    for copy in state_copies:
-        copy.wait_recv()
+    await_all("offset", offset_in.at[:7])
+    pass_on(2)
+
+    await_all("state", state_in.at[:7])
     carry = initial
     for source in range(NZ - 1):
         arrived = state_in[jnp.maximum(z - source, 1)]
@@ -466,20 +471,18 @@
         scan_own[b] = (0.5 * read * (1.0 + jnp.tanh(inner))).astype(BF16)
         carry = falls[b] * turned(gain_block, carry) + ends[b]
 
-    def spread_copies(own, landing, s_sem, r_sem):
-        return {
-            (dx, dy): remote(
-                own.at[(y + dy) % NY], landing.at[dx, dy], s_sem.at[dx, dy], r_sem.at[dx, dy],
-                {"fs": (x + dx) % NX, "sp_1": (y + dy) % NY},
-            )
-            for dx in order for dy in (1, 3, 2, 0) if (dx, dy) != (0, 0)
-        }
-
-    scan_copies = spread_copies(scan_own, scan_in, s_scan, r_scan)
-    for copy in scan_copies.values():
-        send(copy)
+    for dx in order:
+        for dy in (1, 3, 2, 0):
+            if (dx, dy) != (0, 0):
+                send(
+                    remote(
+                        scan_own.at[(y + dy) % NY], scan_in.at[dx, dy], s_of["scan"],
+                        r_of["scan"], {"fs": (x + dx) % NX, "sp_1": (y + dy) % NY},
+                    )
+                )
     scan_in[0, 0] = scan_own[y]
-    pass_slice(2)
+    arrive(2, (2, 3))
+    attend_step(1)
     arrive(3, (0, 1))
     attend_step(2)
     arrive(3, (2, 3))
@@ -496,82 +499,81 @@
         join(0, dz)
     for dz in (6, 7):
         join(5, dz)
-    arrive(4)
-    attend_far(4, far_in)
-    for dz in (4, 5):
-        join(0, dz)
-    attend_own[...] = acc[0].astype(BF16).reshape(NY, 128, 128)
-    attend_copies = [
-        send(
-            remote(
-                attend_own.at[(y + dy) % NY], attend_in.at[:, column], s_attend.at[dy],
-                r_attend.at[dy], {"sp_1": (y + dy) % NY},
-            )
-        )
-        for dy in (1, 3, 2)
-    ]
-    attend_in[:, column] = attend_own[y]
-
-    part_copies = {}
+    other = pl.ds(pl.multiple_of((1 - t) * 64, 64), 64)
+    await_all("scan", drive_w.at[:1920])
     for dx in order:
         total = None
         for dy in range(NY):
-            if (dx, dy) != (0, 0):
-                scan_copies[dx, dy].wait_recv()
             head = (y + NY - dy) % NY
             head_rows = pl.ds(pl.multiple_of(head * 128, 128), 128)
             product = jnp.dot(scan_in[dx, dy], w_scan[head_rows, :], preferred_element_type=F32)
             total = product if total is None else total + product
-        rounded = total.astype(BF16)
-        for k in range(NT):
-            part_out[dx, k] = rounded[k * 64 : (k + 1) * 64]
-        for dt in range(NT):
-            if (dx, dt) != (0, 0):
-                to = (t + dt) % NT
-                part_copies[dx, dt] = send(
-                    remote(
-                        part_out.at[dx, to], part_in.at[dx, dt], s_part.at[dx, dt],
-                        r_part.at[dx, dt], {"fs": (x + NX - dx) % NX, "tp": to},
-                    )
-                )
-    part_in[0, 0] = part_out[0, t]
+        scan_product[dx] = total
+        pre_out[dx] = scan_product[dx, other, :].astype(BF16)
+        send(remote(pre_out.at[dx], pre_in.at[dx], s_of["pre"], r_of["pre"], sibling))
+    arrive(4)
+    attend_far(4, far_in)
+    await_all("pre", pre_in)
     for dx in (1, 3, 2):
-        for dy in (1, 3, 2):
-            relay_copy(dx, dy).wait_recv()
-    for copy in attend_copies:
-        copy.wait_recv()
-    other = pl.ds(pl.multiple_of((1 - t) * 64, 64), 64)
-    last_copies = []
+        part_out[dx] = (scan_product[dx, mine, :] + pre_in[dx].astype(F32)).astype(BF16)
+        send(
+            remote(
+                part_out.at[dx], part_in.at[dx], s_of["part"], r_of["part"],
+                {"fs": (x + NX - dx) % NX},
+            )
+        )
+    for dz in (4, 5):
+        join(0, dz)
+    attend_own[...] = acc[0].astype(BF16).reshape(NY, 128, 128)
+    for dy in (1, 3, 2):
+        send(
+            remote(
+                attend_own.at[(y + dy) % NY], attend_in.at[:, column], s_of["attend"],
+                r_of["attend"], {"sp_1": (y + dy) % NY},
+            )
+        )
+    attend_in[:, column] = attend_own[y]
+
+    await_all("hop", w_attend.at[0, :384])
+    await_all("attend", drive_w.at[:384])
     for k in range(NX):
         product_own[k] = jnp.dot(attend_in[...], w_attend[k], preferred_element_type=F32)
         half_out[k] = product_own[k, other, :].astype(BF16)
-        last_copies.append(
-            send(remote(half_out.at[k], half_in.at[k], s_last.at[k], r_last.at[k], sibling))
-        )
-    for copy in last_copies:
-        copy.wait_recv()
+        send(remote(half_out.at[k], half_in.at[k], s_of["last"], r_of["last"], sibling))
+    await_all("last", half_in)
+    await_all("part", w_attend.at[0, :192])
     for dx in order:
-        for dt in range(NT):
-            if (dx, dt) != (0, 0):
-                part_copies[dx, dt].wait_recv()
         k = (x + dx) % NX
         columns = pl.ds(pl.multiple_of(k * 512, 512), 512)
-        scan_part = part_in[dx, 0].astype(F32) + part_in[dx, 1].astype(F32)
+        scan_part = scan_product[0, mine, :] + pre_in[0].astype(F32)
+        if dx:
+            scan_part = part_in[dx].astype(F32)
         out[:, columns] = (product_own[k, mine, :] + half_in[k].astype(F32) + scan_part).astype(BF16)
-    for copy in sent:
-        copy.wait_send()
-    for i in range(1, 5):
-        for j in range(NY):
-            if i < 4 or j < 2:
-                right_copy(i, j).wait_send()
-            if i < 4 or j >= 2:
-                left_copy(i, j).wait_send()
+    for name, data in {
+        "rows": rows_in.at[:3, :64],
+        "half": rows_in.at[:2],
+        "keyed": keyed_w.at[:1536],
+        "query": query_w.at[:1536],
+        "packed": packed_in.at[:3],
+        "right": w_attend.at[:2, :448],
+        "left": w_attend.at[:2, :448],
+        "offset": offset_in.at[:7],
+        "state": state_in.at[:7],
+        "scan": drive_w.at[:1920],
+        "pre": pre_in,
+        "part": w_attend.at[0, :192],
+        "slice": w_attend.at[0, :384],
+        "relay": w_attend.at[:3, :256],
+        "hop": w_attend.at[0, :384],
+        "attend": drive_w.at[:384],
+        "last": half_in,
+        "drive": drive_w.at[:192],
+        "share": drive_w.at[:1344],
+    }.items():
+        remote(data, data, s_of[name], r_rows.at[0], sibling).wait_send()
 
 
 def layer(*operands):
-    def sems(*shape):
-        return [pltpu.SemaphoreType.DMA(shape)] * 2
-
     return pl.pallas_call(
         layer_kernel,
         out_shape=pltpu.VMEM((64, 2048), BF16),
@@ -616,14 +618,20 @@
             pltpu.VMEM((NY, 128, 128), BF16),
             pltpu.VMEM((128, 512), BF16),
             pltpu.VMEM((NX, NY, 128, 128), BF16),
-            pltpu.VMEM((NX, NT, 64, 512), BF16),
-            pltpu.VMEM((NX, NT, 64, 512), BF16),
+            pltpu.VMEM((NX, 64, 512), BF16),
+            pltpu.VMEM((NX, 64, 512), BF16),
             pltpu.VMEM((NX, 128, 512), F32),
             pltpu.VMEM((NX, 64, 512), BF16),
             pltpu.VMEM((NX, 64, 512), BF16),
-            *sems(NY), *sems(NY), *sems(3, NX), *sems(NY), *sems(4, NY), *sems(4, NY), *sems(NZ),
-            *sems(NZ), *sems(NX, NY), *sems(NX, NT), *sems(NX), *sems(NX, NY), *sems(NY), *sems(NX),
-            *sems(NX), *sems(NX, NZ),
+            pltpu.VMEM((NX, 128, 512), F32),
+            pltpu.VMEM((NX, 64, 512), BF16),
+            pltpu.VMEM((NX, 64, 512), BF16),
+            *(
+                pltpu.SemaphoreType.DMA(shape)
+                for shape in (
+                    (len(SENT),), (len(TOGETHER),), (3,), (14,), (14,), (3,), (3, 2), (3,)
+                )
+            ),
         ],
         compiler_params=pltpu.CompilerParams(
             collective_id=0, has_side_effects=True, vmem_limit_bytes=60 << 20

time: 65.7 us -> 60.2 us (0.916)
  Pallas kernels: 65 us -> 59.4 us
    pallas_call x1, Pallas kernels: 65 us -> 59.4 us  [layer(): pl.pallas_call(layer_kernel, out_shape=pltpu.VMEM((64, 2048), BF16), in_s...]
where the time goes in v7:
time: 60.2 us; the launch traced here: 60.1 us
  Pallas kernels  59.4 us (99%)
  local copies, waits for them, and re-layouts  0.71 us (1%)
    pallas_call x1, Pallas kernels, layer(): pl.pallas_call(layer_kernel, out_shape=pltpu.VMEM((64, 2048), BF16), in_s...  59.4 us

profile of v7, /device:TPU:1, one launch (start us, length us, event | category | flops | bytes accessed | tf_op | source)
XLA Modules:
  0.0 60.1 jit_solution(14563434731057895949)
XLA Ops:
  0.0 59.4 %layer.1 = bf16[64,2048]{1,0:T(8,128)(2,1)S(1)} custom-call(bf16[64,2048]{1,0:T(8,128)(2,1)} %bitcast.11, f32[1,2048]{1,0:T(1,128)} %bitcast.14, bf16[512,512]{1,0:T(8,128)(2,1)} %refs_2_.1, bf16[512,512]{1,0:T(8,128)(2,1)} %refs_3_.1, bf16[512,512]{1,0:T(8,128)(2,1)} %refs_4_.1, bf16[512,512]{1,0:T(8,128)(2,1)} %refs_5_.1, bf16[4,128]{1,0:T(4,128)(2,1)} %bitcast.16, ...), custom_call_target="tpu_custom_call" | custom-call | tf_op jit(solution)/shard_map/layer/pallas_call | solution.py:577
  59.4 0.7 %copy.19 = bf16[1,64,2048]{2,1,0:T(8,128)(2,1)} copy(bf16[1,64,2048]{2,1,0:T(8,128)(2,1)S(1)} %bitcast.9) | data formatting | bytes 524288

commit v8 on v7

--- a/solution.py
+++ b/solution.py
@@ -16,7 +16,7 @@
 BF16, F32 = jnp.bfloat16, jnp.float32
 TOGETHER = (
     "half", "keyed", "query", "packed", "offset", "state", "scan", "pre", "part", "hop", "attend",
-    "last", "share",
+    "last", "share", "far_rows", "values",
 )
 SENT = TOGETHER + ("rows", "right", "left", "slice", "relay", "drive")
 VMEM = pl.BlockSpec(memory_space=pltpu.VMEM)
@@ -144,9 +144,19 @@
     mine = pl.ds(pl.multiple_of(t * 64, 64), 64)
     sibling = {"tp": 1 - t}
 
-    def row_copy(j):
-        return remote(
-            normed, rows_in.at[j, mine], s_of["rows"], r_rows.at[j - 1],
+    def quarter(half):
+        return pl.ds(pl.multiple_of(t * 64 + half * 32, 32), 32)
+
+    def row_copy(j, half):
+        return remote(
+            normed.at[pl.ds(half * 32, 32)], rows_in.at[j, quarter(half)], s_of["rows"],
+            r_rows.at[2 * j - 2 + half], {"sp_1": (y + order[j]) % NY},
+        )
+
+    def far_row_copy(j):
+        part = quarter(j - 1)
+        return remote(
+            rows_in.at[j, part], rows_in.at[3, part], s_of["far_rows"], r_of["far_rows"],
             {"sp_1": (y + order[j]) % NY},
         )
 
@@ -176,6 +186,19 @@
             w_drive.at[pl.ds(pl.multiple_of(z * 64, 64), 64), column], eighth(x), s_of["drive"],
             r_drive.at[dx - 1], {"fs": (x + dx) % NX},
         )
+
+    def value_eighth(k):
+        return keyed_w.at[pl.ds(pl.multiple_of(k * 512 + z * 64, 64), 64), 128:]
+
+    def value_copy():
+        return remote(
+            w_value.at[pl.ds(pl.multiple_of(z * 64, 64), 64), column], value_eighth(x),
+            s_of["drive"], r_drive.at[3], {"fs": (x + 2) % NX},
+        )
+
+    def value_share_copy(dz):
+        part = value_eighth((x + 2) % NX)
+        return remote(part, part, s_of["values"], r_of["values"], {"sp_0": (z + dz) % NZ})
 
     def share_copy(dx, dz):
         part = eighth((x + NX - dx) % NX)
@@ -210,13 +233,20 @@
             )
         )
     send(half_copy(0))
-    for j in (1, 2, 3):
-        send(row_copy(j))
+    for half in (0, 1):
+        send(row_copy(1, half))
+        send(row_copy(2, 1 - half))
+    send(value_copy())
+    for dx in (2, 1, 3):
+        send(drive_copy(dx))
+    for dx in (2, 1, 3):
+        send(weight_copy(0, dx))
+    for dx in (1, 3):
+        send(weight_copy(1, dx))
     for dx in (1, 3, 2):
-        send(drive_copy(dx))
-    for kind in (0, 1, None, 2):
-        for dx in (1, 3, 2):
-            send(slice_copy(dx) if kind is None else weight_copy(kind, dx))
+        send(slice_copy(dx))
+    for dx in (2, 1, 3):
+        send(weight_copy(2, dx))
     packed_in[y] = packed[y]
     rows_in[0, mine] = normed[...]
     keyed_w[depth, :128] = w_key[:, column]
@@ -324,9 +354,12 @@
                 {"sp_0": (z + dz) % NZ},
             )
         )
-    for dx in (1, 3, 2):
+    value_copy().wait_recv()
+    for dz in (4, 3, 5, 2, 6, 1, 7):
+        send(value_share_copy(dz))
+    for dx in (2, 1, 3):
         drive_copy(dx).wait_recv()
-        for dz in (1, 7, 2, 6, 3, 5, 4):
+        for dz in (4, 3, 5, 2, 6, 1, 7):
             send(share_copy(dx, dz))
     until = jnp.where(lane <= row, 1.0, 0.0)
     until_half = until.astype(BF16)
@@ -341,10 +374,15 @@
             precision=lax.Precision.HIGHEST,
         )
         falls.append(jnp.sum(forget, axis=1, keepdims=True))
-    for j in (1, 2, 3):
-        row_copy(j).wait_recv()
-        send(half_copy(j))
-    await_all("keyed", keyed_w.at[:1536])
+    for half in (0, 1):
+        row_copy(1, half).wait_recv()
+        row_copy(2, 1 - half).wait_recv()
+        for j in (1, 2):
+            send(half_copy(j) if half else far_row_copy(j))
+    await_all("far_rows", rows_in.at[3, :64])
+    send(half_copy(3))
+    await_all("keyed", keyed_w.at[:1280])
+    await_all("values", drive_w.at[:448])
     await_all("half", rows_in.at[:2])
     product = jnp.dot(
         rows_in[...].reshape(512, 2048), keyed_w[...], preferred_element_type=F32
@@ -389,6 +427,8 @@
             relay_copy(dx, dy).wait_recv()
             send(hop_copy(dx, dy))
 
+    pass_slice(1)
+    arrive(1, (0,))
     await_all("share", drive_w.at[:1344])
     product = jnp.dot(
         rows_in[...].reshape(512, 2048), drive_w[...], preferred_element_type=F32
@@ -414,10 +454,9 @@
         ends[b] = falls[b] * turned(gain_last, ends[b])
         local = falls[b] * turned(gain_block, local) + ends[b]
         if b == 1:
-            pass_slice(1)
-        elif b > 1:
-            arrive(1, (b - 2,))
-    pass_slice(3)
+            pass_slice(3)
+        if b < 3:
+            arrive(1, (b + 1,))
     state_own[:8, :] = local
     state_own[8:, :] = jnp.broadcast_to(fall_all, (8, 128))
     for dz in range(1, NZ):
@@ -428,7 +467,6 @@
             )
         )
 
-    arrive(1, (2, 3))
     pass_slice(2)
     pass_on(1)
     await_all("query", query_w.at[:1536])
@@ -471,8 +509,8 @@
         scan_own[b] = (0.5 * read * (1.0 + jnp.tanh(inner))).astype(BF16)
         carry = falls[b] * turned(gain_block, carry) + ends[b]
 
-    for dx in order:
-        for dy in (1, 3, 2, 0):
+    for dx in (2, 1, 3, 0):
+        for dy in (2, 1, 3, 0):
             if (dx, dy) != (0, 0):
                 send(
                     remote(
@@ -513,8 +551,19 @@
         send(remote(pre_out.at[dx], pre_in.at[dx], s_of["pre"], r_of["pre"], sibling))
     arrive(4)
     attend_far(4, far_in)
+    for dz in (4, 5):
+        join(0, dz)
+    attend_own[...] = acc[0].astype(BF16).reshape(NY, 128, 128)
+    for dy in (2, 1, 3):
+        send(
+            remote(
+                attend_own.at[(y + dy) % NY], attend_in.at[:, column], s_of["attend"],
+                r_of["attend"], {"sp_1": (y + dy) % NY},
+            )
+        )
+    attend_in[:, column] = attend_own[y]
     await_all("pre", pre_in)
-    for dx in (1, 3, 2):
+    for dx in (2, 1, 3):
         part_out[dx] = (scan_product[dx, mine, :] + pre_in[dx].astype(F32)).astype(BF16)
         send(
             remote(
@@ -522,17 +571,6 @@
                 {"fs": (x + NX - dx) % NX},
             )
         )
-    for dz in (4, 5):
-        join(0, dz)
-    attend_own[...] = acc[0].astype(BF16).reshape(NY, 128, 128)
-    for dy in (1, 3, 2):
-        send(
-            remote(
-                attend_own.at[(y + dy) % NY], attend_in.at[:, column], s_of["attend"],
-                r_of["attend"], {"sp_1": (y + dy) % NY},
-            )
-        )
-    attend_in[:, column] = attend_own[y]
 
     await_all("hop", w_attend.at[0, :384])
     await_all("attend", drive_w.at[:384])
@@ -550,9 +588,11 @@
             scan_part = part_in[dx].astype(F32)
         out[:, columns] = (product_own[k, mine, :] + half_in[k].astype(F32) + scan_part).astype(BF16)
     for name, data in {
-        "rows": rows_in.at[:3, :64],
+        "rows": rows_in.at[:2, :64],
         "half": rows_in.at[:2],
-        "keyed": keyed_w.at[:1536],
+        "keyed": keyed_w.at[:1280],
+        "values": drive_w.at[:448],
+        "far_rows": rows_in.at[3, :64],
         "query": query_w.at[:1536],
         "packed": packed_in.at[:3],
         "right": w_attend.at[:2, :448],
@@ -567,7 +607,7 @@
         "hop": w_attend.at[0, :384],
         "attend": drive_w.at[:384],
         "last": half_in,
-        "drive": drive_w.at[:192],
+        "drive": drive_w.at[:256],
         "share": drive_w.at[:1344],
     }.items():
         remote(data, data, s_of[name], r_rows.at[0], sibling).wait_send()
@@ -629,7 +669,7 @@
             *(
                 pltpu.SemaphoreType.DMA(shape)
                 for shape in (
-                    (len(SENT),), (len(TOGETHER),), (3,), (14,), (14,), (3,), (3, 2), (3,)
+                    (len(SENT),), (len(TOGETHER),), (4,), (14,), (14,), (3,), (3, 2), (4,)
                 )
             ),
         ],

time: 60.2 us -> 59.7 us (level)
  no operation moved by 1% of the time
where the time goes in v8:
time: 59.7 us
  Pallas kernels  59 us (99%)
  local copies, waits for them, and re-layouts  0.71 us (1%)
    pallas_call x1, Pallas kernels, layer(): pl.pallas_call(layer_kernel, out_shape=pltpu.VMEM((64, 2048), BF16), in_s...  59 us

profile of v8, /device:TPU:1, one launch (start us, length us, event | category | flops | bytes accessed | tf_op | source)
XLA Modules:
  0.0 59.7 jit_solution(6257465814688659080)
XLA Ops:
  0.0 59.0 %layer.1 = bf16[64,2048]{1,0:T(8,128)(2,1)S(1)} custom-call(bf16[64,2048]{1,0:T(8,128)(2,1)} %bitcast.11, f32[1,2048]{1,0:T(1,128)} %bitcast.14, bf16[512,512]{1,0:T(8,128)(2,1)} %refs_2_.1, bf16[512,512]{1,0:T(8,128)(2,1)} %refs_3_.1, bf16[512,512]{1,0:T(8,128)(2,1)} %refs_4_.1, bf16[512,512]{1,0:T(8,128)(2,1)} %refs_5_.1, bf16[4,128]{1,0:T(4,128)(2,1)} %bitcast.16, ...), custom_call_target="tpu_custom_call" | custom-call | tf_op jit(solution)/shard_map/layer/pallas_call | solution.py:617
  59.0 0.7 %copy.19 = bf16[1,64,2048]{2,1,0:T(8,128)(2,1)} copy(bf16[1,64,2048]{2,1,0:T(8,128)(2,1)S(1)} %bitcast.9) | data formatting | bytes 524288

commit v9 on v8

--- a/solution.py
+++ b/solution.py
@@ -428,7 +428,6 @@
             send(hop_copy(dx, dy))
 
     pass_slice(1)
-    arrive(1, (0,))
     await_all("share", drive_w.at[:1344])
     product = jnp.dot(
         rows_in[...].reshape(512, 2048), drive_w[...], preferred_element_type=F32
@@ -455,8 +454,9 @@
         local = falls[b] * turned(gain_block, local) + ends[b]
         if b == 1:
             pass_slice(3)
+            pass_slice(2)
         if b < 3:
-            arrive(1, (b + 1,))
+            arrive(1, (b,))
     state_own[:8, :] = local
     state_own[8:, :] = jnp.broadcast_to(fall_all, (8, 128))
     for dz in range(1, NZ):
@@ -467,8 +467,10 @@
             )
         )
 
-    pass_slice(2)
+    arrive(1, (3,))
+    arrive(2, (0,))
     pass_on(1)
+    arrive(2, (1,))
     await_all("query", query_w.at[:1536])
     product = jnp.dot(
         rows_in[...].reshape(512, 2048), query_w[...], preferred_element_type=F32
@@ -477,14 +479,18 @@
     for j in range(NY):
         queries[block_of(j)] = product[j * 128 : (j + 1) * 128]
 
-    arrive(2, (0, 1))
-    pass_on(3)
+    arrive(2, (2,))
     acc[0], tot[0] = attend_chunk(
         queries[...].reshape(512, 128), own_in[...].reshape(512, 256), offset_row(0), ladder[...],
         lax.broadcasted_iota(jnp.int32, (512, 512), 1)
         < lax.broadcasted_iota(jnp.int32, (512, 512), 0),
     )
     await_all("offset", offset_in.at[:7])
+    pass_on(3)
+    arrive(2, (3,))
+    arrive(3, (0,))
+    attend_far(1, right_in.at[0])
+    arrive(3, (1,))
     pass_on(2)
 
     await_all("state", state_in.at[:7])
@@ -519,11 +525,10 @@
                     )
                 )
     scan_in[0, 0] = scan_own[y]
-    arrive(2, (2, 3))
-    attend_step(1)
-    arrive(3, (0, 1))
+    arrive(3, (2,))
+    attend_far(7, left_in.at[0])
+    arrive(3, (3,))
     attend_step(2)
-    arrive(3, (2, 3))
     attend_step(3)
 
     def join(near, far):
@@ -537,6 +542,19 @@
         join(0, dz)
     for dz in (6, 7):
         join(5, dz)
+    arrive(4)
+    attend_far(4, far_in)
+    for dz in (4, 5):
+        join(0, dz)
+    attend_own[...] = acc[0].astype(BF16).reshape(NY, 128, 128)
+    for dy in (2, 1, 3):
+        send(
+            remote(
+                attend_own.at[(y + dy) % NY], attend_in.at[:, column], s_of["attend"],
+                r_of["attend"], {"sp_1": (y + dy) % NY},
+            )
+        )
+    attend_in[:, column] = attend_own[y]
     other = pl.ds(pl.multiple_of((1 - t) * 64, 64), 64)
     await_all("scan", drive_w.at[:1920])
     for dx in order:
@@ -549,19 +567,12 @@
         scan_product[dx] = total
         pre_out[dx] = scan_product[dx, other, :].astype(BF16)
         send(remote(pre_out.at[dx], pre_in.at[dx], s_of["pre"], r_of["pre"], sibling))
-    arrive(4)
-    attend_far(4, far_in)
-    for dz in (4, 5):
-        join(0, dz)
-    attend_own[...] = acc[0].astype(BF16).reshape(NY, 128, 128)
-    for dy in (2, 1, 3):
-        send(
-            remote(
-                attend_own.at[(y + dy) % NY], attend_in.at[:, column], s_of["attend"],
-                r_of["attend"], {"sp_1": (y + dy) % NY},
-            )
-        )
-    attend_in[:, column] = attend_own[y]
+    await_all("hop", w_attend.at[0, :384])
+    await_all("attend", drive_w.at[:384])
+    for k in range(NX):
+        product_own[k] = jnp.dot(attend_in[...], w_attend[k], preferred_element_type=F32)
+        half_out[k] = product_own[k, other, :].astype(BF16)
+        send(remote(half_out.at[k], half_in.at[k], s_of["last"], r_of["last"], sibling))
     await_all("pre", pre_in)
     for dx in (2, 1, 3):
         part_out[dx] = (scan_product[dx, mine, :] + pre_in[dx].astype(F32)).astype(BF16)
@@ -571,13 +582,6 @@
                 {"fs": (x + NX - dx) % NX},
             )
         )
-
-    await_all("hop", w_attend.at[0, :384])
-    await_all("attend", drive_w.at[:384])
-    for k in range(NX):
-        product_own[k] = jnp.dot(attend_in[...], w_attend[k], preferred_element_type=F32)
-        half_out[k] = product_own[k, other, :].astype(BF16)
-        send(remote(half_out.at[k], half_in.at[k], s_of["last"], r_of["last"], sibling))
     await_all("last", half_in)
     await_all("part", w_attend.at[0, :192])
     for dx in order:

time: 59.7 us -> 61.5 us (1.030)
  Pallas kernels: 59 us -> 60.7 us
    pallas_call x1, Pallas kernels: 59 us -> 60.7 us  [layer(): pl.pallas_call(layer_kernel, out_shape=pltpu.VMEM((64, 2048), BF16), in_s...]
where the time goes in v9:
time: 61.5 us; the launch traced here: 61.4 us
  Pallas kernels  60.7 us (99%)
  local copies, waits for them, and re-layouts  0.71 us (1%)
    pallas_call x1, Pallas kernels, layer(): pl.pallas_call(layer_kernel, out_shape=pltpu.VMEM((64, 2048), BF16), in_s...  60.7 us

profile of v9, /device:TPU:1, one launch (start us, length us, event | category | flops | bytes accessed | tf_op | source)
XLA Modules:
  0.0 61.4 jit_solution(11840724892424165540)
XLA Ops:
  0.0 60.7 %layer.1 = bf16[64,2048]{1,0:T(8,128)(2,1)S(1)} custom-call(bf16[64,2048]{1,0:T(8,128)(2,1)} %bitcast.11, f32[1,2048]{1,0:T(1,128)} %bitcast.14, bf16[512,512]{1,0:T(8,128)(2,1)} %refs_2_.1, bf16[512,512]{1,0:T(8,128)(2,1)} %refs_3_.1, bf16[512,512]{1,0:T(8,128)(2,1)} %refs_4_.1, bf16[512,512]{1,0:T(8,128)(2,1)} %refs_5_.1, bf16[4,128]{1,0:T(4,128)(2,1)} %bitcast.16, ...), custom_call_target="tpu_custom_call" | custom-call | tf_op jit(solution)/shard_map/layer/pallas_call | solution.py:621
  60.7 0.7 %copy.19 = bf16[1,64,2048]{2,1,0:T(8,128)(2,1)} copy(bf16[1,64,2048]{2,1,0:T(8,128)(2,1)S(1)} %bitcast.9) | data formatting | bytes 524288

commit v10 on v8

--- a/solution.py
+++ b/solution.py
@@ -428,7 +428,6 @@
             send(hop_copy(dx, dy))
 
     pass_slice(1)
-    arrive(1, (0,))
     await_all("share", drive_w.at[:1344])
     product = jnp.dot(
         rows_in[...].reshape(512, 2048), drive_w[...], preferred_element_type=F32
@@ -455,8 +454,9 @@
         local = falls[b] * turned(gain_block, local) + ends[b]
         if b == 1:
             pass_slice(3)
+            pass_slice(2)
         if b < 3:
-            arrive(1, (b + 1,))
+            arrive(1, (b,))
     state_own[:8, :] = local
     state_own[8:, :] = jnp.broadcast_to(fall_all, (8, 128))
     for dz in range(1, NZ):
@@ -467,8 +467,10 @@
             )
         )
 
-    pass_slice(2)
+    arrive(1, (3,))
+    arrive(2, (0,))
     pass_on(1)
+    arrive(2, (1,))
     await_all("query", query_w.at[:1536])
     product = jnp.dot(
         rows_in[...].reshape(512, 2048), query_w[...], preferred_element_type=F32
@@ -477,15 +479,16 @@
     for j in range(NY):
         queries[block_of(j)] = product[j * 128 : (j + 1) * 128]
 
-    arrive(2, (0, 1))
-    pass_on(3)
+    arrive(2, (2,))
     acc[0], tot[0] = attend_chunk(
         queries[...].reshape(512, 128), own_in[...].reshape(512, 256), offset_row(0), ladder[...],
         lax.broadcasted_iota(jnp.int32, (512, 512), 1)
         < lax.broadcasted_iota(jnp.int32, (512, 512), 0),
     )
     await_all("offset", offset_in.at[:7])
+    pass_on(3)
     pass_on(2)
+    arrive(2, (3,))
 
     await_all("state", state_in.at[:7])
     carry = initial
@@ -519,11 +522,14 @@
                     )
                 )
     scan_in[0, 0] = scan_own[y]
-    arrive(2, (2, 3))
-    attend_step(1)
-    arrive(3, (0, 1))
-    attend_step(2)
-    arrive(3, (2, 3))
+    arrive(3, (0,))
+    attend_far(1, right_in.at[0])
+    arrive(3, (1,))
+    attend_far(7, left_in.at[0])
+    arrive(3, (2,))
+    attend_far(2, right_in.at[1])
+    arrive(3, (3,))
+    attend_far(6, left_in.at[1])
     attend_step(3)
 
     def join(near, far):
@@ -571,7 +577,6 @@
                 {"fs": (x + NX - dx) % NX},
             )
         )
-
     await_all("hop", w_attend.at[0, :384])
     await_all("attend", drive_w.at[:384])
     for k in range(NX):

time: 59.7 us -> 59.2 us (level)
  Pallas kernels: 59 us -> 58.4 us
where the time goes in v10:
time: 59.2 us; the launch traced here: 59.1 us
  Pallas kernels  58.4 us (99%)
  local copies, waits for them, and re-layouts  0.71 us (1%)
    pallas_call x1, Pallas kernels, layer(): pl.pallas_call(layer_kernel, out_shape=pltpu.VMEM((64, 2048), BF16), in_s...  58.4 us

profile of v10, /device:TPU:1, one launch (start us, length us, event | category | flops | bytes accessed | tf_op | source)
XLA Modules:
  0.0 59.1 jit_solution(9588770704398189311)
XLA Ops:
  0.0 58.4 %layer.1 = bf16[64,2048]{1,0:T(8,128)(2,1)S(1)} custom-call(bf16[64,2048]{1,0:T(8,128)(2,1)} %bitcast.11, f32[1,2048]{1,0:T(1,128)} %bitcast.14, bf16[512,512]{1,0:T(8,128)(2,1)} %refs_2_.1, bf16[512,512]{1,0:T(8,128)(2,1)} %refs_3_.1, bf16[512,512]{1,0:T(8,128)(2,1)} %refs_4_.1, bf16[512,512]{1,0:T(8,128)(2,1)} %refs_5_.1, bf16[4,128]{1,0:T(4,128)(2,1)} %bitcast.16, ...), custom_call_target="tpu_custom_call" | custom-call | tf_op jit(solution)/shard_map/layer/pallas_call | solution.py:622
  58.4 0.7 %copy.19 = bf16[1,64,2048]{2,1,0:T(8,128)(2,1)} copy(bf16[1,64,2048]{2,1,0:T(8,128)(2,1)S(1)} %bitcast.9) | data formatting | bytes 524288

commit v11 on v10

--- a/solution.py
+++ b/solution.py
@@ -413,6 +413,13 @@
                 ladder[...],
             )
 
+    def join(near, far):
+        @pl.when(z >= far)
+        def _():
+            fallen = tot[near, :, :1]
+            acc[near] += jnp.exp2(fallen) * acc[far]
+            tot[near, :, :1] = fallen + tot[far, :, :1]
+
     def attend_step(i):
         attend_far(i, right_in.at[i - 1])
         attend_far(8 - i, left_in.at[i - 1])
@@ -517,42 +524,30 @@
             if (dx, dy) != (0, 0):
                 send(
                     remote(
-                        scan_own.at[(y + dy) % NY], scan_in.at[dx, dy], s_of["scan"],
+                        scan_own.at[(y + dy) % NY], scan_in.at[dx, :, column], s_of["scan"],
                         r_of["scan"], {"fs": (x + dx) % NX, "sp_1": (y + dy) % NY},
                     )
                 )
-    scan_in[0, 0] = scan_own[y]
+    scan_in[0, :, column] = scan_own[y]
     arrive(3, (0,))
     attend_far(1, right_in.at[0])
+    join(0, 1)
     arrive(3, (1,))
     attend_far(7, left_in.at[0])
     arrive(3, (2,))
     attend_far(2, right_in.at[1])
+    join(0, 2)
     arrive(3, (3,))
     attend_far(6, left_in.at[1])
     attend_step(3)
 
-    def join(near, far):
-        @pl.when(z >= far)
-        def _():
-            fallen = tot[near, :, :1]
-            acc[near] += jnp.exp2(fallen) * acc[far]
-            tot[near, :, :1] = fallen + tot[far, :, :1]
-
-    for dz in (1, 2, 3):
-        join(0, dz)
+    join(0, 3)
     for dz in (6, 7):
         join(5, dz)
     other = pl.ds(pl.multiple_of((1 - t) * 64, 64), 64)
     await_all("scan", drive_w.at[:1920])
     for dx in order:
-        total = None
-        for dy in range(NY):
-            head = (y + NY - dy) % NY
-            head_rows = pl.ds(pl.multiple_of(head * 128, 128), 128)
-            product = jnp.dot(scan_in[dx, dy], w_scan[head_rows, :], preferred_element_type=F32)
-            total = product if total is None else total + product
-        scan_product[dx] = total
+        scan_product[dx] = jnp.dot(scan_in[dx], w_scan[...], preferred_element_type=F32)
         pre_out[dx] = scan_product[dx, other, :].astype(BF16)
         send(remote(pre_out.at[dx], pre_in.at[dx], s_of["pre"], r_of["pre"], sibling))
     arrive(4)
@@ -662,7 +657,7 @@
             pltpu.VMEM((NY, 128, 128), BF16),
             pltpu.VMEM((NY, 128, 128), BF16),
             pltpu.VMEM((128, 512), BF16),
-            pltpu.VMEM((NX, NY, 128, 128), BF16),
+            pltpu.VMEM((NX, 128, 512), BF16),
             pltpu.VMEM((NX, 64, 512), BF16),
             pltpu.VMEM((NX, 64, 512), BF16),
             pltpu.VMEM((NX, 128, 512), F32),

time: 59.2 us -> 59 us (level)
  no operation moved by 1% of the time
where the time goes in v11:
time: 59 us; the launch traced here: 58.9 us
  Pallas kernels  58.2 us (99%)
  local copies, waits for them, and re-layouts  0.71 us (1%)
    pallas_call x1, Pallas kernels, layer(): pl.pallas_call(layer_kernel, out_shape=pltpu.VMEM((64, 2048), BF16), in_s...  58.2 us

profile of v11, /device:TPU:1, one launch (start us, length us, event | category | flops | bytes accessed | tf_op | source)
XLA Modules:
  0.0 58.9 jit_solution(13489443266067366632)
XLA Ops:
  0.0 58.2 %layer.1 = bf16[64,2048]{1,0:T(8,128)(2,1)S(1)} custom-call(bf16[64,2048]{1,0:T(8,128)(2,1)} %bitcast.11, f32[1,2048]{1,0:T(1,128)} %bitcast.14, bf16[512,512]{1,0:T(8,128)(2,1)} %refs_2_.1, bf16[512,512]{1,0:T(8,128)(2,1)} %refs_3_.1, bf16[512,512]{1,0:T(8,128)(2,1)} %refs_4_.1, bf16[512,512]{1,0:T(8,128)(2,1)} %refs_5_.1, bf16[4,128]{1,0:T(4,128)(2,1)} %bitcast.16, ...), custom_call_target="tpu_custom_call" | custom-call | tf_op jit(solution)/shard_map/layer/pallas_call | solution.py:617
  58.2 0.7 %copy.19 = bf16[1,64,2048]{2,1,0:T(8,128)(2,1)} copy(bf16[1,64,2048]{2,1,0:T(8,128)(2,1)S(1)} %bitcast.9) | data formatting | bytes 524288
